TPU v7x, 32 devices: a whole 2x2x4 slice. The times are simulated.
32 devices in a mesh: ep: 4 (over y, x), tp: 8 (over z, core).
Axes of the slice: x: 2, y: 2, z: 4, core: 2. Of those that a mesh axis runs over, the one named last changes fastest.
Arguments:
- receptance: bfloat16 [4096, 1024], P('ep', 'tp'), may hold values from -6 to 6
- key_in: bfloat16 [4096, 1024], P('ep', 'tp'), may hold values from -6 to 6
- payload_vectors: bfloat16 [4096, 1024], P('ep', 'tp'), may hold values from -6 to 6
- decay_in: bfloat16 [4096, 1024], P('ep', 'tp'), may hold values from -30 to 3
- rate_in: bfloat16 [4096, 1024], P('ep', 'tp'), may hold values from -30 to 6
- gate_in: bfloat16 [4096, 1024], P('ep', 'tp'), may hold values from -6 to 6
- norm_gain: float32 [1024], P('tp'), may hold values from 0.1 to 1.9
- out_weight: bfloat16 [1024, 2048], P('tp'), may hold values from -0.1875 to 0.1875
- moe_in: bfloat16 [4096, 2048], P(('ep', 'tp')), may hold values from -6 to 6
- moe_gain: float32 [2048], replicated, may hold values from 0.1 to 1.9
- routes: int32 [4096, 2], P(('ep', 'tp')), may hold values from 0 to 7, all different within a row; in each aligned block of 128 rows (0 to 127, 128 to 255, ...) at most 48 rows name the same one
- route_weights: float32 [4096, 2], P(('ep', 'tp')), may hold values from 0.2 to 1
- expert_gate: bfloat16 [8, 2048, 512], P('ep', None, 'tp'), may hold values from -0.125 to 0.125
- expert_up: bfloat16 [8, 2048, 512], P('ep', None, 'tp'), may hold values from -0.125 to 0.125
- expert_down: bfloat16 [8, 2048, 512], P('ep', None, 'tp'), may hold values from -0.25 to 0.25
- shared_gate: bfloat16 [2048, 512], replicated, may hold values from -0.125 to 0.125
- shared_up: bfloat16 [2048, 512], replicated, may hold values from -0.125 to 0.125
- shared_down: bfloat16 [512, 2048], replicated, may hold values from -0.25 to 0.25
Outputs:
- mixed: bfloat16 [4096, 2048], P(('ep', 'tp'))
- moe_out: bfloat16 [4096, 2048], P(('ep', 'tp'))
Inputs may be any that keep to these rules, and one draw needn't show every extreme that they name: `routes`: each token names 2 different experts; within the rows of one device no expert is named more than 48 times, a bound that some block reaches there.
All inputs are finite; a program needn't handle non-finite values.
Results may differ from a plain program's by a relative error of at most 0.019.
Values may be sent and summed in bfloat16 or wider, within the bound.
A program may use at most 128 MiB of HBM per device.

v0:
```python
import functools

import jax
import jax.numpy as jnp
from jax import lax
from jax.experimental import pallas as pl
from jax.experimental.pallas import tpu as pltpu
from jax.sharding import PartitionSpec as P

HEAD_DIM = 64
BLOCK = 64


def dims(form):
    return {"nn": ((1,), (0,)), "nt": ((1,), (1,)), "tn": ((0,), (0,))}[form]


def mm1(left, right, form="nn"):
    return lax.dot_general(
        left.astype(jnp.bfloat16),
        right.astype(jnp.bfloat16),
        (dims(form), ((), ())),
        preferred_element_type=jnp.float32,
    )


def mm3(left, right, form="nn"):
    lh, rh = left.astype(jnp.bfloat16), right.astype(jnp.bfloat16)
    ll = (left - lh.astype(jnp.float32)).astype(jnp.bfloat16)
    rl = (right - rh.astype(jnp.float32)).astype(jnp.bfloat16)
    return mm1(lh, rh, form) + (mm1(lh, rl, form) + mm1(ll, rh, form))


mm_g = mm3
mm_inv = mm3
mm_q = mm3
mm_out = mm3
mm_car = mm3
mm_scan = mm3


def head_masks(rows, width):
    lane = lax.broadcasted_iota(jnp.int32, (rows, width), 1)
    return lane < HEAD_DIM


def stacked(x):
    first = head_masks(*x.shape)
    return jnp.concatenate([jnp.where(first, x, 0.0), jnp.where(first, 0.0, x)], axis=0)


def per_head_sum(x):
    first = head_masks(*x.shape)
    one = jnp.sum(jnp.where(first, x, 0.0), axis=-1, keepdims=True)
    both = jnp.sum(jnp.where(first, 0.0, x), axis=-1, keepdims=True)
    return jnp.where(first, one, both)


def sigmoid(x):
    return 1.0 / (1.0 + jnp.exp(-x))


def local_block(r_in, k_in, v_in, d_in, b_in):
    f32 = jnp.float32
    keys = k_in.astype(f32)
    unit = keys * lax.rsqrt(per_head_sum(keys * keys) + 1e-06)
    log_decay = sigmoid(d_in.astype(f32)) * -0.6065306597126334
    tri_row = lax.broadcasted_iota(jnp.int32, (BLOCK, 3 * BLOCK), 0)
    tri_col = lax.broadcasted_iota(jnp.int32, (BLOCK, 3 * BLOCK), 1) % BLOCK
    tri = jnp.where(tri_col <= tri_row, 1.0, 0.0).astype(jnp.bfloat16)
    hi = log_decay.astype(jnp.bfloat16)
    rest = log_decay - hi.astype(f32)
    mid = rest.astype(jnp.bfloat16)
    low = (rest - mid.astype(f32)).astype(jnp.bfloat16)
    cumul = mm1(tri, jnp.concatenate([hi, mid, low], axis=0))
    end_scale = jnp.exp(cumul[BLOCK - 1 :, :])
    shrink = jnp.exp(-cumul)
    query2 = stacked(r_in.astype(f32) * jnp.exp(cumul))
    alpha2 = stacked(-unit * jnp.exp(cumul - log_decay))
    key_grow = keys * shrink
    beta_grow = unit * sigmoid(b_in.astype(f32)) * shrink
    values2 = stacked(v_in.astype(f32))
    two = 2 * BLOCK
    grams = mm_g(
        jnp.concatenate([alpha2, query2], axis=0),
        jnp.concatenate([beta_grow, beta_grow, key_grow, key_grow], axis=0),
        "nt",
    )
    row = lax.broadcasted_iota(jnp.int32, (two, two), 0)
    col = lax.broadcasted_iota(jnp.int32, (two, two), 1)
    same = row // BLOCK == col // BLOCK
    strict = same & (col < row)
    inclusive = same & (col <= row)
    couple = jnp.where(strict, grams[:two, :two], 0.0)
    insert = jnp.where(strict, grams[:two, two:], 0.0)
    read_beta = jnp.where(inclusive, grams[two:, :two], 0.0)
    read_key = jnp.where(inclusive, grams[two:, two:], 0.0)
    size = 8
    near = jnp.where(row // size == col // size, couple, 0.0)
    inverse = jnp.where(row == col, 1.0, 0.0) + near
    power = mm_inv(near, near)
    both = mm_inv(jnp.concatenate([inverse, power], axis=0), power)
    inverse = inverse + both[:two]
    inverse = inverse + mm_inv(inverse, both[two:])
    while size < BLOCK:
        wide = 2 * size
        off = jnp.where(
            (row // wide == col // wide) & (row // size != col // size), couple, 0.0
        )
        inverse = inverse + mm_inv(inverse, mm_inv(off, inverse))
        size = wide
    inserted = mm_q(insert, values2)
    qz = mm_q(inverse, jnp.concatenate([alpha2, inserted], axis=1))
    lower = jnp.concatenate([jnp.zeros_like(values2), values2], axis=1)
    stack = jnp.concatenate([qz, lower], axis=0)
    reads = mm_out(jnp.concatenate([read_beta, read_key], axis=1), stack)
    query_bar = query2 + reads[:, :two]
    local_out = reads[:, two:]
    ends = jnp.concatenate([stacked(beta_grow * end_scale), stacked(key_grow * end_scale)], axis=0)
    maps = mm_car(stack, ends, "tn")
    return query_bar, local_out, maps, end_scale


def local_kernel(unroll, r_ref, k_ref, v_ref, d_ref, b_ref, qp_ref, lo_ref, total_ref, state):
    two = 2 * BLOCK
    row = lax.broadcasted_iota(jnp.int32, (2 * two, two), 0)
    col = lax.broadcasted_iota(jnp.int32, (2 * two, two), 1)
    state[...] = jnp.where(row == col, 1.0, 0.0)

    @pl.loop(0, r_ref.shape[0] // (BLOCK * unroll))
    def _(step):
        parts = []
        for u in range(unroll):
            rows = pl.ds(pl.multiple_of((step * unroll + u) * BLOCK, BLOCK), BLOCK)
            parts.append(
                local_block(
                    r_ref[rows, :], k_ref[rows, :], v_ref[rows, :], d_ref[rows, :], b_ref[rows, :]
                )
            )
        now = state[...]
        for u, (query_bar, local_out, maps, end_scale) in enumerate(parts):
            rows = pl.ds(pl.multiple_of((step * unroll + u) * BLOCK, BLOCK), BLOCK)
            out = mm_scan(query_bar, now, "nt")
            qp_ref[rows, :] = out[:BLOCK, :two] + out[BLOCK:, :two]
            lo = out[:, two:] + local_out
            lo_ref[rows, :] = lo[:BLOCK] + lo[BLOCK:]
            moved = mm_scan(now, maps[:two]) + now * end_scale
            now = jnp.concatenate([moved[:two], moved[two:] + maps[two:]], axis=0)
        state[...] = now

    carry, source = state[:two, :], state[two:, :]
    total_ref[0] = (carry[:BLOCK] + carry[BLOCK:]).astype(total_ref.dtype)
    total_ref[1] = (source[:BLOCK] + source[BLOCK:]).astype(total_ref.dtype)


def finish_kernel(groups, qp_ref, lo_ref, all_ref, here_ref, gate_ref, gain_ref, out_ref):
    two = 2 * BLOCK
    here = here_ref[0]
    entry = jnp.zeros((two, two), jnp.float32)
    for k in range(groups):
        carry = stacked(all_ref[k, 0].astype(jnp.float32))
        source = stacked(all_ref[k, 1].astype(jnp.float32))
        entry = jnp.where(k < here, mm3(entry, carry) + source, entry)
    tile = 256 if qp_ref.shape[0] % 256 == 0 else BLOCK

    @pl.loop(0, qp_ref.shape[0] // tile)
    def _(step):
        rows = pl.ds(pl.multiple_of(step * tile, tile), tile)
        recur = mm3(qp_ref[rows, :], entry, "nt") + lo_ref[rows, :]
        centered = recur - per_head_sum(recur) * (1.0 / HEAD_DIM)
        spread = per_head_sum(centered * centered) * (1.0 / HEAD_DIM)
        normed = centered * lax.rsqrt(spread + 0.00064)
        gated = normed * gain_ref[...] * sigmoid(gate_ref[rows, :].astype(jnp.float32))
        out_ref[rows, :] = gated.astype(out_ref.dtype)


def gated_rows(receptance, key_in, payload_vectors, decay_in, rate_in, gate_in, norm_gain):
    length, channels = receptance.shape
    groups = lax.axis_size("ep")
    wide = 2 * HEAD_DIM
    spare = -channels % wide
    pad = lambda x: jnp.pad(x, ((0, 0),) * (x.ndim - 1) + ((0, spare),)) if spare else x
    receptance, key_in, payload_vectors, decay_in, rate_in, gate_in, norm_gain = (
        pad(x)
        for x in (receptance, key_in, payload_vectors, decay_in, rate_in, gate_in, norm_gain)
    )
    pairs = (channels + spare) // wide
    vmem = pl.BlockSpec(memory_space=pltpu.VMEM)
    unroll = 4
    done = []
    for pair in range(pairs):
        cut = slice(pair * wide, (pair + 1) * wide)
        qp, lo, total = pl.pallas_call(
            functools.partial(local_kernel, unroll),
            out_shape=(
                jax.ShapeDtypeStruct((length, wide), jnp.float32),
                jax.ShapeDtypeStruct((length, wide), jnp.float32),
                jax.ShapeDtypeStruct((2, HEAD_DIM, wide), jnp.bfloat16),
            ),
            in_specs=[vmem] * 5,
            out_specs=(vmem, vmem, vmem),
            scratch_shapes=[pltpu.VMEM((2 * wide, wide), jnp.float32)],
            cost_estimate=pl.CostEstimate(
                flops=2 * length * wide * wide * 60, bytes_accessed=4 << 20, transcendentals=0
            ),
        )(
            receptance[:, cut],
            key_in[:, cut],
            payload_vectors[:, cut],
            decay_in[:, cut],
            rate_in[:, cut],
        )
        everything = lax.all_gather(total, "ep")
        done.append(
            pl.pallas_call(
                functools.partial(finish_kernel, groups),
                out_shape=jax.ShapeDtypeStruct((length, wide), jnp.bfloat16),
                in_specs=[vmem] * 3 + [pl.BlockSpec(memory_space=pltpu.SMEM)] + [vmem] * 2,
                out_specs=vmem,
                cost_estimate=pl.CostEstimate(
                    flops=2 * length * wide * wide * 4, bytes_accessed=2 << 20, transcendentals=0
                ),
            )(
                qp,
                lo,
                everything,
                lax.axis_index("ep").reshape(1).astype(jnp.int32),
                gate_in[:, cut],
                norm_gain[cut].reshape(1, wide),
            )
        )
    rows = done[0] if pairs == 1 else jnp.concatenate(done, axis=1)
    return rows[:, :channels]


def expert_layer(
    moe_in,
    moe_gain,
    routes,
    route_weights,
    expert_gate,
    expert_up,
    expert_down,
    shared_gate,
    shared_up,
    shared_down,
):
    tokens, width = moe_in.shape
    top_count = routes.shape[1]
    local_count = expert_gate.shape[0]
    groups = lax.axis_size("ep")
    experts = local_count * groups
    slots = max(2, 3 * tokens * top_count // (2 * experts))
    values = moe_in.astype(jnp.float32)
    centered = values - jnp.mean(values, -1, keepdims=True)
    rescaled_input = (
        centered * lax.rsqrt(jnp.mean(centered * centered, -1, keepdims=True) + 1e-05) * moe_gain
    ).astype(jnp.bfloat16)
    flat = routes.reshape(-1)
    picks = (flat[:, None] == jnp.arange(experts, dtype=jnp.int32)[None, :]).astype(jnp.int32)
    earlier = jnp.cumsum(picks, axis=0) - picks
    rank = jnp.sum(earlier * picks, axis=1)
    slot_index = flat % local_count * (groups * slots) + flat // local_count * slots + rank
    total_slots = local_count * groups * slots
    match = slot_index[:, None] == jnp.arange(total_slots, dtype=jnp.int32)[None, :]
    owner = jnp.arange(tokens * top_count, dtype=jnp.int32) // top_count
    slot_token = jnp.sum(jnp.where(match, owner[:, None], 0), axis=0)
    filled = jnp.any(match, axis=0)
    outgoing = jnp.where(filled[:, None], rescaled_input[slot_token], jnp.zeros((), jnp.bfloat16))
    outgoing = outgoing.reshape(local_count, groups, slots, width)
    arrived = lax.all_to_all(outgoing, "ep", split_axis=1, concat_axis=1, tiled=True).reshape(
        local_count, groups * slots, width
    )
    shared_gate_out = jnp.dot(rescaled_input, shared_gate, preferred_element_type=jnp.float32)
    shared_up_out = jnp.dot(rescaled_input, shared_up, preferred_element_type=jnp.float32)
    shared_hidden = (jax.nn.silu(shared_gate_out) * shared_up_out).astype(jnp.bfloat16)
    shared_term = jnp.dot(shared_hidden, shared_down, preferred_element_type=jnp.float32)
    gate_whole, up_whole, down_whole = (
        lax.all_gather(expert_gate, "tp", axis=2, tiled=True),
        lax.all_gather(expert_up, "tp", axis=2, tiled=True),
        lax.all_gather(expert_down, "tp", axis=2, tiled=True),
    )
    gate = jnp.einsum("erd,edf->erf", arrived, gate_whole, preferred_element_type=jnp.float32)
    upper = jnp.einsum("erd,edf->erf", arrived, up_whole, preferred_element_type=jnp.float32)
    hidden = (jax.nn.silu(gate) * upper).astype(jnp.bfloat16)
    results = jnp.einsum("erf,edf->erd", hidden, down_whole, preferred_element_type=jnp.float32)
    sending = results.astype(jnp.bfloat16).reshape(local_count, groups, slots, width)
    returned = lax.all_to_all(sending, "ep", split_axis=1, concat_axis=1, tiled=True).reshape(
        total_slots, width
    )
    picked = returned[slot_index].reshape(tokens, top_count, width)
    share = 2.5 * route_weights / jnp.sum(route_weights, -1, keepdims=True)
    combined = shared_term + jnp.sum(picked.astype(jnp.float32) * share[:, :, None], axis=1)
    return combined.astype(jnp.bfloat16)


def shards(
    receptance,
    key_in,
    payload_vectors,
    decay_in,
    rate_in,
    gate_in,
    norm_gain,
    out_weight,
    moe_in,
    moe_gain,
    routes,
    route_weights,
    expert_gate,
    expert_up,
    expert_down,
    shared_gate,
    shared_up,
    shared_down,
):
    mixer_rows = gated_rows(
        receptance, key_in, payload_vectors, decay_in, rate_in, gate_in, norm_gain
    )
    token_rows = lax.all_to_all(mixer_rows, "tp", split_axis=0, concat_axis=1, tiled=True)
    mixed = jnp.dot(
        token_rows,
        lax.all_gather(out_weight, "tp", axis=0, tiled=True),
        preferred_element_type=jnp.float32,
    )
    moe_out = expert_layer(
        moe_in,
        moe_gain,
        routes,
        route_weights,
        expert_gate,
        expert_up,
        expert_down,
        shared_gate,
        shared_up,
        shared_down,
    )
    return (mixed.astype(jnp.bfloat16), moe_out)


def solution(mesh):
    placed = (
        P("ep", "tp"),
        P("ep", "tp"),
        P("ep", "tp"),
        P("ep", "tp"),
        P("ep", "tp"),
        P("ep", "tp"),
        P("tp"),
        P("tp", None),
        P(("ep", "tp"), None),
        P(),
        P(("ep", "tp"), None),
        P(("ep", "tp"), None),
        P("ep", None, "tp"),
        P("ep", None, "tp"),
        P("ep", None, "tp"),
        P(),
        P(),
        P(),
    )
    return jax.shard_map(
        shards,
        mesh=mesh,
        in_specs=placed,
        out_specs=(P(("ep", "tp"), None), P(("ep", "tp"), None)),
        check_vma=False,
    )
```

profile of v0, /device:TPU:0, one launch (start us, length us, event | category | flops | bytes accessed | tf_op | source)
XLA Modules:
  0.0 237.5 jit_solution(8271830576337192595)
XLA Ops:
  7.3 0.7 all-gather.8.cloned.1.call-update
  8.0 0.7 all-gather.10.cloned.1.call-update
  8.7 0.7 all-gather.12.cloned.1.call-update
  9.5 0.5 all-gather.6.cloned.1.call-update
  10.4 0.6 reduce-window.6
  11.0 0.2 slice_reduce_fusion
  11.6 0.2 select_reduce_fusion
  12.0 0.3 fusion.5
  12.3 0.4 fusion.7
  12.7 3.1 %gather_fusion = bf16[384,2048]{1,0:T(8,128)(2,1)} fusion(bf16[128,2048]{1,0:T(8,128)(2,1)S(1)} %fusion.7, s32[1024]{0:T(1024)S(1)} %pad_clamp_fusion.1), kind=kCustom, calls=%fused_computation | custom fusion | bytes 3147264 | tf_op jit(solution)/shard_map/gather | solution.py:269
  15.8 2.7 %copy_select_fusion = bf16[2,4,48,2048]{3,2,0,1:T(8,128)(2,1)} fusion(bf16[2,4,48,2048]{3,2,1,0:T(8,128)(2,1)} %bitcast.36, pred[2,4,48]{2,0,1:T(4,128)(4,1)S(1)} %copy.48), kind=kLoop, calls=%fused_computation.7 | loop fusion | flops 786432 | bytes 3146112 | tf_op jit(solution)/shard_map/jit(_where)/select_n | solution.py:269
  18.5 5.2 %all-to-all-start.1 = ((bf16[2,4,48,2048]{3,2,0,1:T(8,128)(2,1)}), bf16[2,4,48,2048]{3,2,0,1:T(8,128)(2,1)}, u32[]{:S(2)}, u32[]{:S(2)}) async-start(bf16[2,4,48,2048]{3,2,0,1:T(8,128)(2,1)} %copy_select_fusion), calls=%async_computation.1 | async-start | bytes 3145728 | tf_op jit(solution)/shard_map/all_to_all | solution.py:271
  23.9 44.8 %shard_map.185 = (f32[1024,128]{1,0:T(8,128)}, f32[1024,128]{1,0:T(8,128)}, bf16[2,64,128]{2,1,0:T(8,128)(2,1)}) custom-call(bf16[1024,128]{1,0:T(8,128)(2,1)} %r_ref.1, bf16[1024,128]{1,0:T(8,128)(2,1)} %k_ref.1, bf16[1024,128]{1,0:T(8,128)(2,1)} %v_ref.1, bf16[1024,128]{1,0:T(8,128)(2,1)} %d_ref.1, bf16[1024,128]{1,0:T(8,128)(2,1)} %b_ref.1), custom_call_target="tpu_custom_call" | custom-call | flops 2013265920 | bytes 4194304 | tf_op jit(solution)/shard_map/pallas_call | solution.py:193
  68.7 10.7 %all-gather = bf16[8,64,128]{2,1,0:T(8,128)(2,1)} all-gather(bf16[2,64,128]{2,1,0:T(8,128)(2,1)} %get-tuple-element.7), channel_id=2, replica_groups=mesh['ep'=4,'tp'=8] {'ep'}, dimensions={0}, use_global_device_ids=true | all-gather | bytes 163840 | tf_op jit(solution)/shard_map/all_gather | solution.py:213
  79.4 4.4 %shard_map.186 = bf16[1024,128]{1,0:T(8,128)(2,1)} custom-call(f32[1024,128]{1,0:T(8,128)} %get-tuple-element.5.qp_ref, f32[1024,128]{1,0:T(8,128)} %get-tuple-element.6.lo_ref, bf16[4,2,64,128]{3,2,1,0:T(8,128)(2,1)} %bitcast.40, s32[1]{0:T(128)} %bitcast.1.here_ref, bf16[1024,128]{1,0:T(8,128)(2,1)} %gate_ref.1, f32[1,128]{1,0:T(1,128)} %bitcast.43), custom_call_target="tpu_custom_call" | custom-call | flops 134217728 | bytes 2097152 | tf_op jit(solution)/shard_map/pallas_call | solution.py:215
  83.8 1.8 copy.45
  85.6 5.4 %all-to-all-start = ((bf16[8,128,128]{1,2,0:T(8,128)(2,1)}), bf16[8,128,128]{1,2,0:T(8,128)(2,1)S(1)}, u32[]{:S(2)}, u32[]{:S(2)}) async-start(bf16[8,128,128]{1,2,0:T(8,128)(2,1)} %copy.45), calls=%async_computation | async-start | bytes 524288 | tf_op jit(solution)/shard_map/all_to_all | solution.py:320
  91.0 2.7 %copy.50 = bf16[2,4,48,2048]{3,2,1,0:T(8,128)(2,1)} copy(bf16[2,4,48,2048]{3,2,0,1:T(8,128)(2,1)} %all-to-all-done.1) | data formatting | bytes 3145728 | tf_op jit(solution)/shard_map/all_to_all | solution.py:271
  93.7 5.1 %fusion.34 = f32[2,192,512]{2,1,0:T(8,128)} fusion(bf16[2,192,2048]{2,1,0:T(8,128)(2,1)} %bitcast.34, bf16[2,2048,512]{1,2,0:T(8,128)(2,1)} %all-gather.8.cloned.1.call-done), kind=kOutput, calls=%fused_computation.72 | convolution fusion | flops 805306368 | bytes 6553600 | tf_op jit(solution)/shard_map/erd,edf->erf/dot_general | solution.py:283
  98.9 13.4 %all-gather.10.cloned.1.call-done = bf16[2,2048,512]{1,2,0:T(8,128)(2,1)} async-done(((bf16[2,2048,64]{1,2,0:T(8,128)(2,1)}), bf16[2,2048,512]{1,2,0:T(8,128)(2,1)}) %all-gather.10.cloned.1.call-update) | async-done | bytes 4194320 | tf_op jit(solution)/shard_map/all_gather | solution.py:280
  112.3 47.4 %all-gather.12.cloned.1.call-done = bf16[2,2048,512]{1,2,0:T(8,128)(2,1)} async-done(((bf16[2,2048,64]{1,2,0:T(8,128)(2,1)}), bf16[2,2048,512]{1,2,0:T(8,128)(2,1)}) %all-gather.12.cloned.1.call-update) | async-done | bytes 4194320 | tf_op jit(solution)/shard_map/all_gather | solution.py:281
  159.7 7.8 %convolution_convert_fusion = bf16[2,192,2048]{2,1,0:T(8,128)(2,1)} fusion(bf16[2,2048,512]{1,2,0:T(8,128)(2,1)} %all-gather.12.cloned.1.call-done, bf16[2,192,2048]{2,1,0:T(8,128)(2,1)} %bitcast.35, bf16[2,2048,512]{1,2,0:T(8,128)(2,1)} %all-gather.10.cloned.1.call-done, f32[2,192,512]{2,1,0:T(8,128)} %fusion.34), kind=kOutput, calls=%fused_computation.2 | convolution fusion | flops 1612578816 | bytes 12320768 | tf_op jit(solution)/shard_map/erf,edf->erd/dot_general | solution.py:286
  167.5 3.0 %copy.51 = bf16[2,4,48,2048]{3,2,0,1:T(8,128)(2,1)} copy(bf16[2,4,48,2048]{3,2,1,0:T(8,128)(2,1)} %bitcast.37) | data formatting | bytes 3145728 | tf_op jit(solution)/shard_map/reshape | solution.py:287
  170.5 4.4 %all-to-all-start.2 = ((bf16[2,4,48,2048]{3,2,0,1:T(8,128)(2,1)}), bf16[2,4,48,2048]{3,2,0,1:T(8,128)(2,1)}, u32[]{:S(2)}, u32[]{:S(2)}) async-start(bf16[2,4,48,2048]{3,2,0,1:T(8,128)(2,1)} %copy.51), calls=%async_computation.2 | async-start | bytes 3145728 | tf_op jit(solution)/shard_map/all_to_all | solution.py:288
  175.0 2.1 fusion.33
  177.1 29.8 %all-gather.6.cloned.1.call-done = bf16[1024,2048]{1,0:T(8,128)(2,1)} async-done(((bf16[128,2048]{1,0:T(8,128)(2,1)}), bf16[1024,2048]{1,0:T(8,128)(2,1)}) %all-gather.6.cloned.1.call-update) | async-done | bytes 4194320 | tf_op jit(solution)/shard_map/all_gather | solution.py:323
  206.9 3.7 %convolution_convert_fusion.1 = bf16[128,2048]{1,0:T(8,128)(2,1)} fusion(bf16[128,1024]{0,1:T(8,128)(2,1)S(1)} %bitcast.38, bf16[1024,2048]{1,0:T(8,128)(2,1)} %all-gather.6.cloned.1.call-done), kind=kOutput, calls=%fused_computation.5 | convolution fusion | flops 537133056 | bytes 4980736 | tf_op jit(solution)/shard_map/dot_general | solution.py:321
  210.6 2.7 %copy.52 = bf16[2,4,48,2048]{3,2,1,0:T(8,128)(2,1)} copy(bf16[2,4,48,2048]{3,2,0,1:T(8,128)(2,1)} %all-to-all-done.2) | data formatting | bytes 3145728 | tf_op jit(solution)/shard_map/all_to_all | solution.py:288
  213.4 5.0 %gather_fusion.1 = bf16[256,2048]{1,0:T(8,128)(2,1)} fusion(bf16[384,2048]{1,0:T(8,128)(2,1)} %bitcast.33, s32[1024]{0:T(1024)S(1)} %pad_clamp_fusion), kind=kCustom, calls=%fused_computation.1 | custom fusion | bytes 2098176 | tf_op jit(solution)/shard_map/gather | solution.py:291
  218.3 3.4 %reshape.241 = f32[128,2,2048]{2,1,0:T(2,128)} reshape(bf16[256,2048]{1,0:T(8,128)(2,1)} %gather_fusion.1) | data formatting | bytes 3145728 | tf_op jit(solution)/shard_map/convert_element_type | solution.py:293
  221.7 5.7 %multiply_reduce_fusion = f32[128,2048]{1,0:T(8,128)} fusion(f32[128,2,2048]{2,1,0:T(2,128)} %reshape.241, f32[128,2]{1,0:T(8,128)S(1)} %copy.54), kind=kLoop, calls=%fused_computation.6 | loop fusion | flops 786432 | bytes 3146752 | tf_op jit(solution)/shard_map/reduce_sum | solution.py:293
  227.5 3.5 %fusion = bf16[128,2048]{1,0:T(8,128)(2,1)} fusion(f32[128,2048]{1,0:T(8,128)} %multiply_reduce_fusion, bf16[512,2048]{1,0:T(8,128)(2,1)S(1)} %copy-done, bf16[128,2048]{1,0:T(8,128)(2,1)S(1)} %fusion.7, bf16[2048,512]{1,0:T(8,128)(2,1)} %param.34, f32[128,512]{1,0:T(8,128)S(1)} %fusion.33), kind=kOutput, calls=%fused_computation.4 | convolution fusion | flops 537788416 | bytes 6553600 | tf_op jit(solution)/shard_map/dot_general | solution.py:277
  (40 shorter events, 1.5 us)
Async XLA Ops:
  7.2 220.3 %copy-start = (bf16[512,2048]{1,0:T(8,128)(2,1)S(1)}, bf16[512,2048]{1,0:T(8,128)(2,1)}, u32[]{:S(2)}) copy-start(bf16[512,2048]{1,0:T(8,128)(2,1)} %param.35) | copy-start | bytes 6291460
  7.2 2.8 %copy-start.4 = (s32[128,2]{0,1:T(2,128)S(1)}, s32[128,2]{0,1:T(2,128)}, u32[]{:S(2)}) copy-start(s32[128,2]{0,1:T(2,128)} %param.28) | copy-start | bytes 3076
  7.2 4.6 %copy-start.1 = (bf16[128,2048]{1,0:T(8,128)(2,1)S(1)}, bf16[128,2048]{1,0:T(8,128)(2,1)}, u32[]{:S(2)}) copy-start(bf16[128,2048]{1,0:T(8,128)(2,1)} %param.26) | copy-start | bytes 1572868
  7.2 5.1 %copy-start.2 = (f32[2048]{0:T(1024)S(1)}, f32[2048]{0:T(1024)}, u32[]{:S(2)}) copy-start(f32[2048]{0:T(1024)} %param.27) | copy-start | bytes 24580
  7.2 86.5 %all-gather.8.cloned.1.call-start = ((), (), s32[]{:S(2)}) async-start(), calls=%async_computation.4 | async-start | bytes 4718592 | tf_op jit(solution)/shard_map/all_gather | solution.py:279
  7.9 104.4 %all-gather.10.cloned.1.call-start = ((), (), s32[]{:S(2)}) async-start(), calls=%async_computation.5 | async-start | bytes 4718592 | tf_op jit(solution)/shard_map/all_gather | solution.py:280
  8.7 151.1 %all-gather.12.cloned.1.call-start = ((), (), s32[]{:S(2)}) async-start(), calls=%async_computation.6 | async-start | bytes 4718592 | tf_op jit(solution)/shard_map/all_gather | solution.py:281
  9.4 197.5 %all-gather.6.cloned.1.call-start = ((), (), s32[]{:S(2)}) async-start(), calls=%async_computation.3 | async-start | bytes 4718592 | tf_op jit(solution)/shard_map/all_gather | solution.py:323
  18.5 67.1 %all-to-all-start.1 = ((bf16[2,4,48,2048]{3,2,0,1:T(8,128)(2,1)}), bf16[2,4,48,2048]{3,2,0,1:T(8,128)(2,1)}, u32[]{:S(2)}, u32[]{:S(2)}) async-start(bf16[2,4,48,2048]{3,2,0,1:T(8,128)(2,1)} %copy_select_fusion), calls=%async_computation.1 | async-start | bytes 3145728 | tf_op jit(solution)/shard_map/all_to_all | solution.py:271
  68.7 16.9 %copy-start.3 = (f32[128,2]{0,1:T(2,128)S(1)}, f32[128,2]{0,1:T(2,128)}, u32[]{:S(2)}) copy-start(f32[128,2]{0,1:T(2,128)} %param.29) | copy-start | bytes 3076
  85.6 84.9 %all-to-all-start = ((bf16[8,128,128]{1,2,0:T(8,128)(2,1)}), bf16[8,128,128]{1,2,0:T(8,128)(2,1)S(1)}, u32[]{:S(2)}, u32[]{:S(2)}) async-start(bf16[8,128,128]{1,2,0:T(8,128)(2,1)} %copy.45), calls=%async_computation | async-start | bytes 524288 | tf_op jit(solution)/shard_map/all_to_all | solution.py:320
  170.5 40.1 %all-to-all-start.2 = ((bf16[2,4,48,2048]{3,2,0,1:T(8,128)(2,1)}), bf16[2,4,48,2048]{3,2,0,1:T(8,128)(2,1)}, u32[]{:S(2)}, u32[]{:S(2)}) async-start(bf16[2,4,48,2048]{3,2,0,1:T(8,128)(2,1)} %copy.51), calls=%async_computation.2 | async-start | bytes 3145728 | tf_op jit(solution)/shard_map/all_to_all | solution.py:288
Sparse Core Ops, SparseCore 0:
  9.6 49.7 all-gather.7
  61.1 51.1 all-gather.9
  113.9 45.7 all-gather.11
  161.2 45.6 all-gather.5
where the time goes:
time: 238 us; the launch traced here: 237 us
  waiting for transfers between devices  93.3 us (39%)
  Pallas kernels  49.3 us (21%)
  local copies, waits for them, and re-layouts  22.7 us (10%)
  matrix products  22.2 us (9%)
  starting transfers between devices  15.1 us (6%)
  between operations  13.9 us (6%)
  blocking collectives  10.7 us (4%)
  other arithmetic  10.4 us (4%)
    all_gather x1, waiting for transfers between devices, expert_layer(): lax.all_gather(expert_down, 'tp', axis=2, tiled=True)  47.4 us
    pallas_call x1, Pallas kernels, gated_rows(): pl.pallas_call(functools.partial(local_kernel, unroll), out_shape=(jax.Sh...  44.8 us
    all_gather x1, waiting for transfers between devices, shards(): lax.all_gather(out_weight, 'tp', axis=0, tiled=True)  29.8 us
    all_gather x1, waiting for transfers between devices, expert_layer(): lax.all_gather(expert_up, 'tp', axis=2, tiled=True)  13.4 us
    all_gather x1, blocking collectives, gated_rows(): everything = lax.all_gather(total, 'ep')  10.7 us
    dot_general x1, matrix products, expert_layer(): jnp.einsum('erf,edf->erd', hidden, down_whole, preferred_element_type=jnp...  7.78 us
    reduce_sum x1, other arithmetic, expert_layer(): jnp.sum(picked.astype(jnp.float32) * share[:, :, None], axis=1)  5.72 us
    all_to_all x1, starting transfers between devices, shards(): lax.all_to_all(mixer_rows, 'tp', split_axis=0, concat_axis=1, tiled=True)  5.36 us
  transfers between devices with their start and end apart: 7, of which 3 were waited for; matrix products, arithmetic and copies ran while one was open for 15% of the time, Pallas kernels for 21%

commit v1 on v0

--- a/solution.py
+++ b/solution.py
@@ -121,14 +121,126 @@
     return query_bar, local_out, maps, end_scale
 
 
-def local_kernel(unroll, r_ref, k_ref, v_ref, d_ref, b_ref, qp_ref, lo_ref, total_ref, state):
+def mixer_kernel(
+    unroll,
+    groups,
+    ring,
+    r_ref,
+    k_ref,
+    v_ref,
+    d_ref,
+    b_ref,
+    gate_ref,
+    gain_ref,
+    weight_ref,
+    token_ref,
+    whole_ref,
+    state,
+    qp_ref,
+    lo_ref,
+    rows_ref,
+    totals,
+    ring_send,
+    ring_recv,
+    pair_send,
+    pair_recv,
+    ep_send,
+    ep_recv,
+    row_send,
+    row_recv,
+    own_sem,
+):
     two = 2 * BLOCK
+    peers = 2 * ring
+    here, mine = lax.axis_index("ep"), lax.axis_index("tp")
+    depth, core = mine // 2, mine % 2
+    partner = depth * 2 + 1 - core
+    after = (depth + 1) % ring * 2 + core
+    before = (depth + ring - 1) % ring * 2 + core
+    chunks, height = weight_ref.shape[0], weight_ref.shape[1]
+    kinds = chunks // 2
+    span = peers * height
+    tokens = token_ref.shape[0]
+    MESH = pl.DeviceIdType.MESH
+
+    def place(chunk, origin):
+        last = chunk // (chunks - 2)
+        base = (1 - last) * (chunk * span + origin * height) + last * (
+            (chunks - 2) * span + origin * 2 * height + (chunk - chunks + 2) * height
+        )
+        return whole_ref.at[pl.ds(pl.multiple_of(base, height), height), :]
+
+    def ring_copy(source, chunk, origin, step, target):
+        return pltpu.make_async_remote_copy(
+            src_ref=source,
+            dst_ref=place(chunk, origin),
+            send_sem=ring_send.at[chunk, step],
+            recv_sem=ring_recv.at[chunk, step],
+            device_id={"tp": target},
+            device_id_type=MESH,
+        )
+
+    def pair_copy(source, chunk, origin, step):
+        return pltpu.make_async_remote_copy(
+            src_ref=source,
+            dst_ref=place(chunk, origin),
+            send_sem=pair_send.at[chunk, step],
+            recv_sem=pair_recv.at[chunk, step],
+            device_id={"tp": partner},
+            device_id_type=MESH,
+        )
+
+    def own_copy(chunk):
+        return pltpu.make_async_copy(
+            weight_ref.at[chunk], place(chunk, mine), own_sem.at[chunk]
+        )
+
+    barrier = pltpu.get_barrier_semaphore()
+    for q in range(1, peers):
+        pl.semaphore_signal(
+            barrier, inc=1, device_id={"tp": (mine + q) % peers}, device_id_type=MESH
+        )
+    for q in range(1, groups):
+        pl.semaphore_signal(
+            barrier, inc=1, device_id={"ep": (here + q) % groups}, device_id_type=MESH
+        )
+    pl.semaphore_wait(barrier, peers + groups - 2)
+
+    def begin(kind, carry):
+        for way, target in ((0, after), (1, before)):
+            chunk = kind * 2 + way
+            ring_copy(weight_ref.at[chunk], chunk, mine, 0, target).start()
+            pair_copy(weight_ref.at[chunk], chunk, mine, 0).start()
+            own_copy(chunk).start()
+        return carry
+
+    lax.fori_loop(0, kinds, begin, 0)
+
+    def relay(k, carry):
+        hop, kind = k // kinds + 1, k % kinds
+        for way, target in ((0, after), (1, before)):
+            chunk = kind * 2 + way
+            shift = ring - hop if way == 0 else hop
+            origin = (depth + shift) % ring * 2 + core
+            block = place(chunk, origin)
+            ring_copy(block, chunk, origin, hop - 1, target).wait_recv()
+
+            @pl.when(hop < ring - 1)
+            def _():
+                ring_copy(block, chunk, origin, hop, target).start()
+
+            pair_copy(block, chunk, origin, hop).start()
+        return carry
+
     row = lax.broadcasted_iota(jnp.int32, (2 * two, two), 0)
     col = lax.broadcasted_iota(jnp.int32, (2 * two, two), 1)
     state[...] = jnp.where(row == col, 1.0, 0.0)
-
-    @pl.loop(0, r_ref.shape[0] // (BLOCK * unroll))
-    def _(step):
+    turns = r_ref.shape[0] // (BLOCK * unroll)
+    relays = (ring - 1) * kinds
+    each = 2
+    inside = min(turns, relays // each)
+
+    def turn(step, carry):
         parts = []
         for u in range(unroll):
             rows = pl.ds(pl.multiple_of((step * unroll + u) * BLOCK, BLOCK), BLOCK)
@@ -148,89 +260,160 @@
             now = jnp.concatenate([moved[:two], moved[two:] + maps[two:]], axis=0)
         state[...] = now
 
-    carry, source = state[:two, :], state[two:, :]
-    total_ref[0] = (carry[:BLOCK] + carry[BLOCK:]).astype(total_ref.dtype)
-    total_ref[1] = (source[:BLOCK] + source[BLOCK:]).astype(total_ref.dtype)
-
-
-def finish_kernel(groups, qp_ref, lo_ref, all_ref, here_ref, gate_ref, gain_ref, out_ref):
-    two = 2 * BLOCK
-    here = here_ref[0]
-    entry = jnp.zeros((two, two), jnp.float32)
-    for k in range(groups):
-        carry = stacked(all_ref[k, 0].astype(jnp.float32))
-        source = stacked(all_ref[k, 1].astype(jnp.float32))
-        entry = jnp.where(k < here, mm3(entry, carry) + source, entry)
-    tile = 256 if qp_ref.shape[0] % 256 == 0 else BLOCK
-
-    @pl.loop(0, qp_ref.shape[0] // tile)
-    def _(step):
-        rows = pl.ds(pl.multiple_of(step * tile, tile), tile)
+        @pl.when(step < inside)
+        def _():
+            lax.fori_loop(step * each, (step + 1) * each, relay, 0)
+
+        return carry
+
+    lax.fori_loop(0, turns, turn, 0)
+
+    carry_map, source_map = state[:two, :], state[two:, :]
+    totals[here, 0] = (carry_map[:BLOCK] + carry_map[BLOCK:]).astype(totals.dtype)
+    totals[here, 1] = (source_map[:BLOCK] + source_map[BLOCK:]).astype(totals.dtype)
+
+    def ep_copy(q, slot):
+        return pltpu.make_async_remote_copy(
+            src_ref=totals.at[slot],
+            dst_ref=totals.at[slot],
+            send_sem=ep_send.at[q],
+            recv_sem=ep_recv.at[q],
+            device_id={"ep": (here + q) % groups},
+            device_id_type=MESH,
+        )
+
+    for q in range(1, groups):
+        ep_copy(q, here).start()
+    for q in range(1, groups):
+        ep_copy(q, (here + groups - q) % groups).wait_recv()
+
+    def enter(k, entry):
+        carry = stacked(totals[k, 0].astype(jnp.float32))
+        source = stacked(totals[k, 1].astype(jnp.float32))
+        reached = jnp.where(k < here, 1.0, 0.0)
+        return entry + reached * (mm3(entry, carry) + source - entry)
+
+    entry = lax.fori_loop(0, groups, enter, jnp.zeros((two, two), jnp.float32))
+    entry = entry.astype(jnp.float32)
+
+    def row_copy(q, target, source):
+        return pltpu.make_async_remote_copy(
+            src_ref=rows_ref.at[pl.ds(pl.multiple_of(target * tokens, tokens), tokens), :],
+            dst_ref=token_ref.at[:, pl.ds(pl.multiple_of(source * two, two), two)],
+            send_sem=row_send.at[q],
+            recv_sem=row_recv.at[q],
+            device_id={"tp": target},
+            device_id_type=MESH,
+        )
+
+    def finish(rows):
         recur = mm3(qp_ref[rows, :], entry, "nt") + lo_ref[rows, :]
         centered = recur - per_head_sum(recur) * (1.0 / HEAD_DIM)
         spread = per_head_sum(centered * centered) * (1.0 / HEAD_DIM)
         normed = centered * lax.rsqrt(spread + 0.00064)
         gated = normed * gain_ref[...] * sigmoid(gate_ref[rows, :].astype(jnp.float32))
-        out_ref[rows, :] = gated.astype(out_ref.dtype)
-
-
-def gated_rows(receptance, key_in, payload_vectors, decay_in, rate_in, gate_in, norm_gain):
+        rows_ref[rows, :] = gated.astype(rows_ref.dtype)
+
+    def finish_turn(q, carry):
+        target = (mine + q) % peers
+        finish(pl.ds(pl.multiple_of(target * tokens, tokens), tokens))
+        return carry
+
+    lax.fori_loop(0, peers, finish_turn, 0)
+    own = rows_ref.at[pl.ds(pl.multiple_of(mine * tokens, tokens), tokens), :]
+    own_rows = pltpu.make_async_copy(
+        own, token_ref.at[:, pl.ds(pl.multiple_of(mine * two, two), two)], own_sem.at[chunks]
+    )
+    own_rows.start()
+
+    def row_start(q, carry):
+        row_copy(q, (mine + q) % peers, mine).start()
+        return carry
+
+    lax.fori_loop(1, peers, row_start, 0)
+
+    lax.fori_loop(inside * each, relays, relay, 0)
+
+    def close(chunk, carry):
+        own_copy(chunk).wait()
+
+        def shut(hop, inner):
+            pair_copy(weight_ref.at[chunk], chunk, mine, hop).wait()
+            return inner
+
+        def shut_ring(hop, inner):
+            ring_copy(weight_ref.at[chunk], chunk, mine, hop, after).wait_send()
+            return inner
+
+        lax.fori_loop(0, ring, shut, 0)
+        lax.fori_loop(0, ring - 1, shut_ring, 0)
+        return carry
+
+    lax.fori_loop(0, chunks, close, 0)
+    own_rows.wait()
+
+    def row_end(q, carry):
+        row_copy(q, (mine + q) % peers, (mine + peers - q) % peers).wait()
+        return carry
+
+    lax.fori_loop(1, peers, row_end, 0)
+    for q in range(1, groups):
+        ep_copy(q, here).wait_send()
+
+
+def mixer_and_weights(
+    receptance, key_in, payload_vectors, decay_in, rate_in, gate_in, norm_gain, weights
+):
     length, channels = receptance.shape
-    groups = lax.axis_size("ep")
+    groups, peers = lax.axis_size("ep"), lax.axis_size("tp")
+    ring = peers // 2
     wide = 2 * HEAD_DIM
-    spare = -channels % wide
+    spare = wide - channels
     pad = lambda x: jnp.pad(x, ((0, 0),) * (x.ndim - 1) + ((0, spare),)) if spare else x
-    receptance, key_in, payload_vectors, decay_in, rate_in, gate_in, norm_gain = (
-        pad(x)
-        for x in (receptance, key_in, payload_vectors, decay_in, rate_in, gate_in, norm_gain)
-    )
-    pairs = (channels + spare) // wide
+    chunks, height, width = weights.shape
     vmem = pl.BlockSpec(memory_space=pltpu.VMEM)
-    unroll = 4
-    done = []
-    for pair in range(pairs):
-        cut = slice(pair * wide, (pair + 1) * wide)
-        qp, lo, total = pl.pallas_call(
-            functools.partial(local_kernel, unroll),
-            out_shape=(
-                jax.ShapeDtypeStruct((length, wide), jnp.float32),
-                jax.ShapeDtypeStruct((length, wide), jnp.float32),
-                jax.ShapeDtypeStruct((2, HEAD_DIM, wide), jnp.bfloat16),
-            ),
-            in_specs=[vmem] * 5,
-            out_specs=(vmem, vmem, vmem),
-            scratch_shapes=[pltpu.VMEM((2 * wide, wide), jnp.float32)],
-            cost_estimate=pl.CostEstimate(
-                flops=2 * length * wide * wide * 60, bytes_accessed=4 << 20, transcendentals=0
-            ),
-        )(
-            receptance[:, cut],
-            key_in[:, cut],
-            payload_vectors[:, cut],
-            decay_in[:, cut],
-            rate_in[:, cut],
-        )
-        everything = lax.all_gather(total, "ep")
-        done.append(
-            pl.pallas_call(
-                functools.partial(finish_kernel, groups),
-                out_shape=jax.ShapeDtypeStruct((length, wide), jnp.bfloat16),
-                in_specs=[vmem] * 3 + [pl.BlockSpec(memory_space=pltpu.SMEM)] + [vmem] * 2,
-                out_specs=vmem,
-                cost_estimate=pl.CostEstimate(
-                    flops=2 * length * wide * wide * 4, bytes_accessed=2 << 20, transcendentals=0
-                ),
-            )(
-                qp,
-                lo,
-                everything,
-                lax.axis_index("ep").reshape(1).astype(jnp.int32),
-                gate_in[:, cut],
-                norm_gain[cut].reshape(1, wide),
-            )
-        )
-    rows = done[0] if pairs == 1 else jnp.concatenate(done, axis=1)
-    return rows[:, :channels]
+    dma = pltpu.SemaphoreType.DMA
+    tokens, whole = pl.pallas_call(
+        functools.partial(mixer_kernel, 4, groups, ring),
+        out_shape=(
+            jax.ShapeDtypeStruct((length // peers, peers * wide), jnp.bfloat16),
+            jax.ShapeDtypeStruct((chunks * peers * height, width), jnp.bfloat16),
+        ),
+        in_specs=[vmem] * 8,
+        out_specs=(vmem, pl.BlockSpec(memory_space=pl.ANY)),
+        scratch_shapes=[
+            pltpu.VMEM((2 * wide, wide), jnp.float32),
+            pltpu.VMEM((length, wide), jnp.float32),
+            pltpu.VMEM((length, wide), jnp.float32),
+            pltpu.VMEM((length, wide), jnp.bfloat16),
+            pltpu.VMEM((groups, 2, HEAD_DIM, wide), jnp.bfloat16),
+            dma((chunks, ring)),
+            dma((chunks, ring)),
+            dma((chunks, ring)),
+            dma((chunks, ring)),
+            dma((groups,)),
+            dma((groups,)),
+            dma((peers,)),
+            dma((peers,)),
+            dma((chunks + 1,)),
+        ],
+        compiler_params=pltpu.CompilerParams(collective_id=0, has_side_effects=True),
+        cost_estimate=pl.CostEstimate(
+            flops=2 * length * wide * wide * 200, bytes_accessed=32 << 20, transcendentals=0
+        ),
+    )(
+        pad(receptance),
+        pad(key_in),
+        pad(payload_vectors),
+        pad(decay_in),
+        pad(rate_in),
+        pad(gate_in),
+        pad(norm_gain).reshape(1, wide),
+        weights,
+    )
+    if spare:
+        tokens = tokens.reshape(-1, peers, wide)[:, :, :channels].reshape(-1, peers * channels)
+    return tokens, whole
 
 
 def expert_layer(
@@ -238,16 +421,14 @@
     moe_gain,
     routes,
     route_weights,
-    expert_gate,
-    expert_up,
-    expert_down,
+    local_count,
+    whole,
     shared_gate,
     shared_up,
     shared_down,
 ):
     tokens, width = moe_in.shape
     top_count = routes.shape[1]
-    local_count = expert_gate.shape[0]
     groups = lax.axis_size("ep")
     experts = local_count * groups
     slots = max(2, 3 * tokens * top_count // (2 * experts))
@@ -275,15 +456,11 @@
     shared_up_out = jnp.dot(rescaled_input, shared_up, preferred_element_type=jnp.float32)
     shared_hidden = (jax.nn.silu(shared_gate_out) * shared_up_out).astype(jnp.bfloat16)
     shared_term = jnp.dot(shared_hidden, shared_down, preferred_element_type=jnp.float32)
-    gate_whole, up_whole, down_whole = (
-        lax.all_gather(expert_gate, "tp", axis=2, tiled=True),
-        lax.all_gather(expert_up, "tp", axis=2, tiled=True),
-        lax.all_gather(expert_down, "tp", axis=2, tiled=True),
-    )
-    gate = jnp.einsum("erd,edf->erf", arrived, gate_whole, preferred_element_type=jnp.float32)
-    upper = jnp.einsum("erd,edf->erf", arrived, up_whole, preferred_element_type=jnp.float32)
+    gate_whole, up_whole, down_whole = whole
+    gate = jnp.einsum("erd,efd->erf", arrived, gate_whole, preferred_element_type=jnp.float32)
+    upper = jnp.einsum("erd,efd->erf", arrived, up_whole, preferred_element_type=jnp.float32)
     hidden = (jax.nn.silu(gate) * upper).astype(jnp.bfloat16)
-    results = jnp.einsum("erf,edf->erd", hidden, down_whole, preferred_element_type=jnp.float32)
+    results = jnp.einsum("erf,efd->erd", hidden, down_whole, preferred_element_type=jnp.float32)
     sending = results.astype(jnp.bfloat16).reshape(local_count, groups, slots, width)
     returned = lax.all_to_all(sending, "ep", split_axis=1, concat_axis=1, tiled=True).reshape(
         total_slots, width
@@ -314,23 +491,24 @@
     shared_up,
     shared_down,
 ):
-    mixer_rows = gated_rows(
-        receptance, key_in, payload_vectors, decay_in, rate_in, gate_in, norm_gain
-    )
-    token_rows = lax.all_to_all(mixer_rows, "tp", split_axis=0, concat_axis=1, tiled=True)
-    mixed = jnp.dot(
-        token_rows,
-        lax.all_gather(out_weight, "tp", axis=0, tiled=True),
-        preferred_element_type=jnp.float32,
-    )
+    local_count, width, part = expert_gate.shape
+    weights = jnp.concatenate(
+        [jnp.swapaxes(w, 1, 2) for w in (expert_gate, expert_up, expert_down)]
+        + [out_weight.reshape(2, part, width)],
+        axis=0,
+    )
+    token_rows, whole = mixer_and_weights(
+        receptance, key_in, payload_vectors, decay_in, rate_in, gate_in, norm_gain, weights
+    )
+    whole = whole.reshape(4, -1, width)
+    mixed = jnp.dot(token_rows, whole[3], preferred_element_type=jnp.float32)
     moe_out = expert_layer(
         moe_in,
         moe_gain,
         routes,
         route_weights,
-        expert_gate,
-        expert_up,
-        expert_down,
+        local_count,
+        [whole[k].reshape(local_count, -1, width) for k in range(3)],
         shared_gate,
         shared_up,
         shared_down,

time: 238 us -> 241 us (1.013)
  Pallas kernels: 49.3 us -> 149 us
  waiting for transfers between devices: 93.3 us -> 14.2 us
  between operations: 13.9 us -> 0.78 us
  blocking collectives: 10.7 us -> 0 us
  local copies, waits for them, and re-layouts: 22.7 us -> 29.1 us
  other arithmetic: 10.4 us -> 16.5 us
  starting transfers between devices: 15.1 us -> 9.88 us
    pallas_call x2 -> x1, Pallas kernels: 49.3 us -> 149 us  [mixer_and_weights(): pl.pallas_call(functools.partial(mixer_kernel, 4, groups, ring), out_shap...]
    all_gather x4 -> x0, waiting for transfers between devices: 90.7 us -> none  [the longest x1 47.4 us: expert_layer(): lax.all_gather(expert_down, 'tp', axis=2, tiled=True)]
    all_to_all x1, waiting for transfers between devices: 0.01 us -> 14.2 us  [expert_layer(): lax.all_to_all(sending, 'ep', split_axis=1, concat_axis=1, tiled=True)]
    all_gather x1 -> x0, blocking collectives: 10.7 us -> none  [gated_rows(): everything = lax.all_gather(total, 'ep')]
    slice x1 -> x2, local copies, waits for them, and re-layouts: 0.22 us -> 9.11 us  [the longest x1 8.9 us: shards(): whole[k].reshape(local_count, -1, width)]
    all_to_all x1 -> x0, starting transfers between devices: 5.36 us -> none  [shards(): lax.all_to_all(mixer_rows, 'tp', split_axis=0, concat_axis=1, tiled=True)]
    concatenate x0 -> x1, other arithmetic: none -> 2.97 us  [shards(): jnp.concatenate([jnp.swapaxes(w, 1, 2) for w in (expert_gate, expert_up,...]
    unnamed x4 -> x0, waiting for transfers between devices: 2.58 us -> none
  transfers between devices with their start and end apart: 7 -> 2, of which waited for: 3 -> 1; matrix products, arithmetic and copies ran while one was open for 15% -> 7% of each run, Pallas kernels for 21% -> 62%
where the time goes in v1:
time: 241 us
  Pallas kernels  149 us (62%)
  local copies, waits for them, and re-layouts  29.1 us (12%)
  matrix products  21.1 us (9%)
  other arithmetic  16.5 us (7%)
  waiting for transfers between devices  14.2 us (6%)
  starting transfers between devices  9.88 us (4%)
    pallas_call x1, Pallas kernels, mixer_and_weights(): pl.pallas_call(functools.partial(mixer_kernel, 4, groups, ring), out_shap...  149 us
    all_to_all x1, waiting for transfers between devices, expert_layer(): lax.all_to_all(sending, 'ep', split_axis=1, concat_axis=1, tiled=True)  14.2 us
    slice x1, local copies, waits for them, and re-layouts, shards(): whole[k].reshape(local_count, -1, width)  8.9 us
    dot_general x1, matrix products, expert_layer(): jnp.einsum('erf,efd->erd', hidden, down_whole, preferred_element_type=jnp...  7.61 us
    reduce_sum x1, other arithmetic, expert_layer(): jnp.sum(picked.astype(jnp.float32) * share[:, :, None], axis=1)  5.72 us
    all_to_all x1, starting transfers between devices, expert_layer(): lax.all_to_all(outgoing, 'ep', split_axis=1, concat_axis=1, tiled=True)  5.32 us
    gather x1, local copies, waits for them, and re-layouts, expert_layer(): picked = returned[slot_index].reshape(tokens, top_count, width)  4.96 us
  transfers between devices with their start and end apart: 2, of which 1 were waited for; matrix products, arithmetic and copies ran while one was open for 7% of the time, Pallas kernels for 62%

profile of v1, /device:TPU:0, one launch (start us, length us, event | category | flops | bytes accessed | tf_op | source)
XLA Modules:
  0.0 240.6 jit_solution(8547670473561149820)
XLA Ops:
  0.6 0.9 copy.42
  1.6 0.1 eq.41
  1.7 0.1 reshape.241
  1.9 1.2 convert_reduce_fusion
  3.1 1.3 fusion.10
  4.4 0.6 reduce-window.6
  5.0 0.2 slice_reduce_fusion
  5.3 0.1 fusion.27
  5.4 0.1 fusion.19
  5.5 0.1 select_reduce_fusion
  5.8 1.4 fusion.12
  7.2 3.1 %gather_fusion = bf16[384,2048]{1,0:T(8,128)(2,1)} fusion(bf16[128,2048]{1,0:T(8,128)(2,1)S(1)} %fusion.12, s32[1024]{0:T(1024)S(1)} %pad_clamp_fusion.1), kind=kCustom, calls=%fused_computation | custom fusion | bytes 3147264 | tf_op jit(solution)/shard_map/gather | solution.py:450
  10.3 2.8 %copy_select_fusion = bf16[2,4,48,2048]{3,2,0,1:T(8,128)(2,1)} fusion(bf16[2,4,48,2048]{3,2,1,0:T(8,128)(2,1)} %bitcast.37, pred[2,4,48]{2,0,1:T(4,128)(4,1)S(1)} %copy.44), kind=kLoop, calls=%fused_computation.10 | loop fusion | flops 786432 | bytes 3146112 | tf_op jit(solution)/shard_map/jit(_where)/select_n | solution.py:450
  13.1 5.3 %all-to-all-start = ((bf16[2,4,48,2048]{3,2,0,1:T(8,128)(2,1)}), bf16[2,4,48,2048]{3,2,0,1:T(8,128)(2,1)}, u32[]{:S(2)}, u32[]{:S(2)}) async-start(bf16[2,4,48,2048]{3,2,0,1:T(8,128)(2,1)} %copy_select_fusion), calls=%async_computation | async-start | bytes 3145728 | tf_op jit(solution)/shard_map/all_to_all | solution.py:452
  18.5 3.0 %pad_maximum_fusion.weight_ref = bf16[8,64,2048]{2,1,0:T(8,128)(2,1)} fusion(bf16[2,64,2048]{2,1,0:T(8,128)(2,1)S(1)} %bitcast.41, bf16[2,64,2048]{2,1,0:T(8,128)(2,1)} %bitcast.42, bf16[2,64,2048]{2,1,0:T(8,128)(2,1)} %bitcast.43, bf16[2,64,2048]{2,1,0:T(8,128)(2,1)} %bitcast.44), kind=kLoop, calls=%fused_computation.8 | loop fusion | flops 3145728 | bytes 4194304 | tf_op jit(solution)/shard_map/concatenate | solution.py:495
  21.4 148.9 %shard_map.185 = (bf16[128,1024]{1,0:T(8,128)(2,1)}, bf16[4096,2048]{1,0:T(8,128)(2,1)}) custom-call(bf16[1024,128]{1,0:T(8,128)(2,1)} %r_ref.1, bf16[1024,128]{1,0:T(8,128)(2,1)} %k_ref.1, bf16[1024,128]{1,0:T(8,128)(2,1)} %v_ref.1, bf16[1024,128]{1,0:T(8,128)(2,1)} %d_ref.1, bf16[1024,128]{1,0:T(8,128)(2,1)} %b_ref.1, bf16[1024,128]{1,0:T(8,128)(2,1)} %gate_ref.1, ...), custom_call_target="tpu_custom_call" | custom-call | flops 6710886400 | bytes 33554432 | tf_op jit(solution)/shard_map/pallas_call | solution.py:376
  170.4 0.1 reshape.246
  170.5 8.9 %fusion.38 = (bf16[1024,2048]{1,0:T(8,128)(2,1)}, bf16[1024,2048]{1,0:T(8,128)(2,1)}, bf16[1024,2048]{1,0:T(8,128)(2,1)}) fusion(bf16[4096,2048]{1,0:T(8,128)(2,1)} %get-tuple-element.5), kind=kLoop, calls=%fused_computation.74 | loop fusion | bytes 25165824 | tf_op jit(solution)/shard_map/slice | solution.py:511
  179.4 1.5 copy.46
  181.0 4.3 %fusion.40 = f32[2,192,512]{2,1,0:T(8,128)S(1)} fusion(bf16[2,192,2048]{2,1,0:T(8,128)(2,1)S(1)} %bitcast.35, bf16[2,512,2048]{2,1,0:T(8,128)(2,1)} %bitcast.34), kind=kOutput, calls=%fused_computation.76 | convolution fusion | flops 805306368 | bytes 6553600 | tf_op jit(solution)/shard_map/erd,efd->erf/dot_general | solution.py:460
  185.3 7.6 %convolution_convert_fusion = bf16[2,192,2048]{2,1,0:T(8,128)(2,1)} fusion(bf16[2,512,2048]{2,1,0:T(8,128)(2,1)} %bitcast.38, bf16[2,192,2048]{2,1,0:T(8,128)(2,1)} %bitcast.36, bf16[2,512,2048]{2,1,0:T(8,128)(2,1)} %bitcast.39, f32[2,192,512]{2,1,0:T(8,128)S(1)} %fusion.40), kind=kOutput, calls=%fused_computation.4 | convolution fusion | flops 1612578816 | bytes 12320768 | tf_op jit(solution)/shard_map/erf,efd->erd/dot_general | solution.py:463
  192.9 2.7 %copy.47 = bf16[2,4,48,2048]{3,2,0,1:T(8,128)(2,1)} copy(bf16[2,4,48,2048]{3,2,1,0:T(8,128)(2,1)} %bitcast.40) | data formatting | bytes 3145728 | tf_op jit(solution)/shard_map/reshape | solution.py:464
  195.6 4.6 %all-to-all-start.1 = ((bf16[2,4,48,2048]{3,2,0,1:T(8,128)(2,1)}), bf16[2,4,48,2048]{3,2,0,1:T(8,128)(2,1)}, u32[]{:S(2)}, u32[]{:S(2)}) async-start(bf16[2,4,48,2048]{3,2,0,1:T(8,128)(2,1)} %copy.47), calls=%async_computation.1 | async-start | bytes 3145728 | tf_op jit(solution)/shard_map/all_to_all | solution.py:465
  200.2 0.1 copy.50
  200.3 2.0 fusion.39
  202.4 3.7 %fusion.3 = bf16[128,2048]{1,0:T(8,128)(2,1)} fusion(bf16[128,1024]{1,0:T(8,128)(2,1)S(1)} %copy-done.4, bf16[4096,2048]{1,0:T(8,128)(2,1)} %get-tuple-element.5), kind=kOutput, calls=%fused_computation.7 | convolution fusion | flops 537133056 | bytes 4980736 | tf_op jit(solution)/shard_map/dot_general | solution.py:504
  206.1 14.2 %all-to-all-done.1 = bf16[2,4,48,2048]{3,2,0,1:T(8,128)(2,1)} async-done(((bf16[2,4,48,2048]{3,2,0,1:T(8,128)(2,1)}), bf16[2,4,48,2048]{3,2,0,1:T(8,128)(2,1)}, u32[]{:S(2)}, u32[]{:S(2)}) %all-to-all-start.1) | async-done | bytes 1572896 | tf_op jit(solution)/shard_map/all_to_all | solution.py:465
  220.3 2.7 %copy.48 = bf16[2,4,48,2048]{3,2,1,0:T(8,128)(2,1)} copy(bf16[2,4,48,2048]{3,2,0,1:T(8,128)(2,1)} %all-to-all-done.1) | data formatting | bytes 3145728 | tf_op jit(solution)/shard_map/all_to_all | solution.py:465
  223.1 5.0 %gather_fusion.1 = bf16[256,2048]{1,0:T(8,128)(2,1)} fusion(bf16[384,2048]{1,0:T(8,128)(2,1)} %bitcast.33, s32[1024]{0:T(1024)S(1)} %pad_clamp_fusion), kind=kCustom, calls=%fused_computation.1 | custom fusion | bytes 2098176 | tf_op jit(solution)/shard_map/gather | solution.py:468
  228.0 3.4 %reshape.247 = f32[128,2,2048]{2,1,0:T(2,128)} reshape(bf16[256,2048]{1,0:T(8,128)(2,1)} %gather_fusion.1) | data formatting | bytes 3145728 | tf_op jit(solution)/shard_map/convert_element_type | solution.py:470
  231.4 5.7 %multiply_reduce_fusion = f32[128,2048]{1,0:T(8,128)} fusion(f32[128,2,2048]{2,1,0:T(2,128)} %reshape.247, f32[128,2]{1,0:T(8,128)S(1)} %copy.50), kind=kLoop, calls=%fused_computation.9 | loop fusion | flops 786432 | bytes 3146752 | tf_op jit(solution)/shard_map/reduce_sum | solution.py:470
  237.1 3.5 %fusion.2 = bf16[128,2048]{1,0:T(8,128)(2,1)} fusion(f32[128,2048]{1,0:T(8,128)} %multiply_reduce_fusion, bf16[512,2048]{1,0:T(8,128)(2,1)S(1)} %copy-done, bf16[128,2048]{1,0:T(8,128)(2,1)S(1)} %fusion.12, bf16[2048,512]{1,0:T(8,128)(2,1)} %param.34, f32[128,512]{1,0:T(8,128)S(1)} %fusion.39), kind=kOutput, calls=%fused_computation.6 | convolution fusion | flops 537788416 | bytes 6553600 | tf_op jit(solution)/shard_map/dot_general | solution.py:458
  (25 shorter events, 0.3 us)
Async XLA Ops:
  0.6 236.5 %copy-start = (bf16[512,2048]{1,0:T(8,128)(2,1)S(1)}, bf16[512,2048]{1,0:T(8,128)(2,1)}, u32[]{:S(2)}) copy-start(bf16[512,2048]{1,0:T(8,128)(2,1)} %param.35) | copy-start | bytes 6291460
  13.1 5.3 %copy-start.2 = (bf16[128,2048]{1,0:T(8,128)(2,1)S(1)}, bf16[128,2048]{1,0:T(8,128)(2,1)}, u32[]{:S(2)}) copy-start(bf16[128,2048]{1,0:T(8,128)(2,1)} %param.25) | copy-start | bytes 1572868
  13.1 166.3 %all-to-all-start = ((bf16[2,4,48,2048]{3,2,0,1:T(8,128)(2,1)}), bf16[2,4,48,2048]{3,2,0,1:T(8,128)(2,1)}, u32[]{:S(2)}, u32[]{:S(2)}) async-start(bf16[2,4,48,2048]{3,2,0,1:T(8,128)(2,1)} %copy_select_fusion), calls=%async_computation | async-start | bytes 3145728 | tf_op jit(solution)/shard_map/all_to_all | solution.py:452
  21.4 149.1 %copy-start.3 = (f32[128,2]{0,1:T(2,128)S(1)}, f32[128,2]{0,1:T(2,128)}, u32[]{:S(2)}) copy-start(f32[128,2]{0,1:T(2,128)} %param.29) | copy-start | bytes 3076
  181.0 4.3 %copy-start.1 = (bf16[2,4,48,2048]{3,2,1,0:T(8,128)(2,1)}, bf16[2,4,48,2048]{3,2,1,0:T(8,128)(2,1)S(1)}, u32[]{:S(2)}) copy-start(bf16[2,4,48,2048]{3,2,1,0:T(8,128)(2,1)S(1)} %copy.46) | copy-start | bytes 4718596
  195.6 24.7 %all-to-all-start.1 = ((bf16[2,4,48,2048]{3,2,0,1:T(8,128)(2,1)}), bf16[2,4,48,2048]{3,2,0,1:T(8,128)(2,1)}, u32[]{:S(2)}, u32[]{:S(2)}) async-start(bf16[2,4,48,2048]{3,2,0,1:T(8,128)(2,1)} %copy.47), calls=%async_computation.1 | async-start | bytes 3145728 | tf_op jit(solution)/shard_map/all_to_all | solution.py:465
  200.2 2.2 copy-start.4

commit v2 on v1

--- a/solution.py
+++ b/solution.py
@@ -416,6 +416,21 @@
     return tokens, whole
 
 
+def silu(x):
+    return x / (1.0 + jnp.exp(-x))
+
+
+def ffn_kernel(x_ref, gate_ref, up_ref, down_ref, out_ref):
+    groups, slots, width = x_ref.shape[0], x_ref.shape[2], x_ref.shape[3]
+    x = x_ref[...].reshape(groups * slots, width)
+    nt = (((1,), (1,)), ((), ()))
+    gate = lax.dot_general(x, gate_ref[0], nt, preferred_element_type=jnp.float32)
+    upper = lax.dot_general(x, up_ref[0], nt, preferred_element_type=jnp.float32)
+    hidden = (silu(gate) * upper).astype(jnp.bfloat16)
+    out = jnp.dot(hidden, down_ref[0], preferred_element_type=jnp.float32)
+    out_ref[...] = out.astype(jnp.bfloat16).reshape(groups, 1, slots, width)
+
+
 def expert_layer(
     moe_in,
     moe_gain,
@@ -432,6 +447,7 @@
     groups = lax.axis_size("ep")
     experts = local_count * groups
     slots = max(2, 3 * tokens * top_count // (2 * experts))
+    slots = -(-slots // 16) * 16
     values = moe_in.astype(jnp.float32)
     centered = values - jnp.mean(values, -1, keepdims=True)
     rescaled_input = (
@@ -441,34 +457,56 @@
     picks = (flat[:, None] == jnp.arange(experts, dtype=jnp.int32)[None, :]).astype(jnp.int32)
     earlier = jnp.cumsum(picks, axis=0) - picks
     rank = jnp.sum(earlier * picks, axis=1)
-    slot_index = flat % local_count * (groups * slots) + flat // local_count * slots + rank
-    total_slots = local_count * groups * slots
-    match = slot_index[:, None] == jnp.arange(total_slots, dtype=jnp.int32)[None, :]
-    owner = jnp.arange(tokens * top_count, dtype=jnp.int32) // top_count
-    slot_token = jnp.sum(jnp.where(match, owner[:, None], 0), axis=0)
-    filled = jnp.any(match, axis=0)
-    outgoing = jnp.where(filled[:, None], rescaled_input[slot_token], jnp.zeros((), jnp.bfloat16))
-    outgoing = outgoing.reshape(local_count, groups, slots, width)
-    arrived = lax.all_to_all(outgoing, "ep", split_axis=1, concat_axis=1, tiled=True).reshape(
-        local_count, groups * slots, width
+    slot_index = (flat * slots + rank).reshape(tokens, top_count)
+    total_slots = experts * slots
+    slot_row = jnp.arange(total_slots, dtype=jnp.int32)[None, :]
+    match = [slot_index[:, k : k + 1] == slot_row for k in range(top_count)]
+    chosen = functools.reduce(jnp.logical_or, match).astype(jnp.bfloat16)
+    outgoing = lax.dot_general(
+        chosen, rescaled_input, (((0,), (0,)), ((), ())), preferred_element_type=jnp.float32
+    ).astype(jnp.bfloat16)
+    outgoing = outgoing.reshape(groups, local_count * slots, width)
+    arrived = lax.all_to_all(outgoing, "ep", split_axis=0, concat_axis=0, tiled=True).reshape(
+        groups, local_count, slots, width
     )
     shared_gate_out = jnp.dot(rescaled_input, shared_gate, preferred_element_type=jnp.float32)
     shared_up_out = jnp.dot(rescaled_input, shared_up, preferred_element_type=jnp.float32)
     shared_hidden = (jax.nn.silu(shared_gate_out) * shared_up_out).astype(jnp.bfloat16)
     shared_term = jnp.dot(shared_hidden, shared_down, preferred_element_type=jnp.float32)
-    gate_whole, up_whole, down_whole = whole
-    gate = jnp.einsum("erd,efd->erf", arrived, gate_whole, preferred_element_type=jnp.float32)
-    upper = jnp.einsum("erd,efd->erf", arrived, up_whole, preferred_element_type=jnp.float32)
-    hidden = (jax.nn.silu(gate) * upper).astype(jnp.bfloat16)
-    results = jnp.einsum("erf,efd->erd", hidden, down_whole, preferred_element_type=jnp.float32)
-    sending = results.astype(jnp.bfloat16).reshape(local_count, groups, slots, width)
-    returned = lax.all_to_all(sending, "ep", split_axis=1, concat_axis=1, tiled=True).reshape(
+    span = whole.shape[1]
+    block = (groups, 1, slots, width)
+    results = pl.pallas_call(
+        ffn_kernel,
+        grid=(local_count,),
+        out_shape=jax.ShapeDtypeStruct((groups, local_count, slots, width), jnp.bfloat16),
+        in_specs=[pl.BlockSpec(block, lambda e: (0, e, 0, 0))]
+        + [
+            pl.BlockSpec((1, span, width), functools.partial(lambda k, e: (k + e, 0, 0), k))
+            for k in (0, local_count, 2 * local_count)
+        ],
+        out_specs=pl.BlockSpec(block, lambda e: (0, e, 0, 0)),
+        cost_estimate=pl.CostEstimate(
+            flops=6 * total_slots * width * span, bytes_accessed=16 << 20, transcendentals=0
+        ),
+    )(arrived, whole, whole, whole)
+    sending = results.reshape(groups, local_count * slots, width)
+    returned = lax.all_to_all(sending, "ep", split_axis=0, concat_axis=0, tiled=True).reshape(
         total_slots, width
     )
-    picked = returned[slot_index].reshape(tokens, top_count, width)
     share = 2.5 * route_weights / jnp.sum(route_weights, -1, keepdims=True)
-    combined = shared_term + jnp.sum(picked.astype(jnp.float32) * share[:, :, None], axis=1)
-    return combined.astype(jnp.bfloat16)
+    spread = sum(jnp.where(match[k], share[:, k : k + 1], 0.0) for k in range(top_count))
+    high = spread.astype(jnp.bfloat16)
+    low = (spread - high.astype(jnp.float32)).astype(jnp.bfloat16)
+    routed = jnp.dot(high, returned, preferred_element_type=jnp.float32) + jnp.dot(
+        low, returned, preferred_element_type=jnp.float32
+    )
+    return (shared_term + routed).astype(jnp.bfloat16)
+
+
+def project_kernel(rows_ref, weight_ref, out_ref):
+    out_ref[...] = jnp.dot(
+        rows_ref[...], weight_ref[...], preferred_element_type=jnp.float32
+    ).astype(out_ref.dtype)
 
 
 def shards(
@@ -500,20 +538,31 @@
     token_rows, whole = mixer_and_weights(
         receptance, key_in, payload_vectors, decay_in, rate_in, gate_in, norm_gain, weights
     )
-    whole = whole.reshape(4, -1, width)
-    mixed = jnp.dot(token_rows, whole[3], preferred_element_type=jnp.float32)
+    mixed = pl.pallas_call(
+        project_kernel,
+        grid=(2,),
+        out_shape=jax.ShapeDtypeStruct((token_rows.shape[0], width), jnp.bfloat16),
+        in_specs=[
+            pl.BlockSpec(token_rows.shape, lambda n: (0, 0)),
+            pl.BlockSpec((token_rows.shape[1], width // 2), lambda n: (3, n)),
+        ],
+        out_specs=pl.BlockSpec((token_rows.shape[0], width // 2), lambda n: (0, n)),
+        cost_estimate=pl.CostEstimate(
+            flops=2 * token_rows.size * width, bytes_accessed=5 << 20, transcendentals=0
+        ),
+    )(token_rows, whole)
     moe_out = expert_layer(
         moe_in,
         moe_gain,
         routes,
         route_weights,
         local_count,
-        [whole[k].reshape(local_count, -1, width) for k in range(3)],
+        whole.reshape(4 * local_count, -1, width),
         shared_gate,
         shared_up,
         shared_down,
     )
-    return (mixed.astype(jnp.bfloat16), moe_out)
+    return (mixed, moe_out)
 
 
 def solution(mesh):

time: 241 us -> 204 us (0.85)
  local copies, waits for them, and re-layouts: 29.1 us -> 1.68 us
  Pallas kernels: 149 us -> 161 us
  other arithmetic: 16.5 us -> 6.8 us
  matrix products: 21.1 us -> 13.1 us
  waiting for transfers between devices: 14.2 us -> 11.2 us
    pallas_call x0 -> x2, Pallas kernels: none -> 11.7 us  [the longest x1 8.15 us: expert_layer(): pl.pallas_call(ffn_kernel, grid=(local_count,), out_shape=jax.ShapeDtypeS...]
    slice x2 -> x1, local copies, waits for them, and re-layouts: 9.11 us -> 0.21 us  [the longest x1 8.9 us: shards(): whole[k].reshape(local_count, -1, width)]
    gather x2 -> x0, local copies, waits for them, and re-layouts: 8.09 us -> none  [the longest x1 4.96 us: expert_layer(): picked = returned[slot_index].reshape(tokens, top_count, width)]
    dot_general x3, matrix products: 15.6 us -> 7.58 us  [the longest x1 2.95 us: expert_layer(): lax.dot_general(chosen, rescaled_input, (((0,), (0,)), ((), ())), preferr...]
    reduce_sum x2 -> x0, other arithmetic: 5.87 us -> none  [the longest x1 5.72 us: expert_layer(): jnp.sum(picked.astype(jnp.float32) * share[:, :, None], axis=1)]
    all_to_all x2 -> x0, local copies, waits for them, and re-layouts: 4.25 us -> none  [the longest x1 2.74 us: expert_layer(): lax.all_to_all(sending, 'ep', split_axis=1, concat_axis=1, tiled=True)]
    convert_element_type x1 -> x0, local copies, waits for them, and re-layouts: 3.39 us -> none  [expert_layer(): picked.astype(jnp.float32) * share[:, :, None]]
    all_to_all x2, waiting for transfers between devices: 14.2 us -> 11.2 us  [the longest x1 11.2 us: expert_layer(): lax.all_to_all(sending, 'ep', split_axis=0, concat_axis=0, tiled=True)]
  transfers between devices with their start and end apart: 2 -> 2, of which waited for: 1 -> 1; matrix products, arithmetic and copies ran while one was open for 7% -> 4% of each run, Pallas kernels for 62% -> 75%
where the time goes in v2:
time: 204 us
  Pallas kernels  161 us (79%)
  matrix products  13.1 us (6%)
  waiting for transfers between devices  11.2 us (5%)
  starting transfers between devices  9.66 us (5%)
  other arithmetic  6.8 us (3%)
    pallas_call x1, Pallas kernels, mixer_and_weights(): pl.pallas_call(functools.partial(mixer_kernel, 4, groups, ring), out_shap...  149 us
    all_to_all x1, waiting for transfers between devices, expert_layer(): lax.all_to_all(sending, 'ep', split_axis=0, concat_axis=0, tiled=True)  11.2 us
    pallas_call x1, Pallas kernels, expert_layer(): pl.pallas_call(ffn_kernel, grid=(local_count,), out_shape=jax.ShapeDtypeS...  8.15 us
    all_to_all x1, starting transfers between devices, expert_layer(): lax.all_to_all(outgoing, 'ep', split_axis=0, concat_axis=0, tiled=True)  5.32 us
    all_to_all x1, starting transfers between devices, expert_layer(): lax.all_to_all(sending, 'ep', split_axis=0, concat_axis=0, tiled=True)  4.34 us
  transfers between devices with their start and end apart: 2, of which 1 were waited for; matrix products, arithmetic and copies ran while one was open for 4% of the time, Pallas kernels for 75%

profile of v2, /device:TPU:0, one launch (start us, length us, event | category | flops | bytes accessed | tf_op | source)
XLA Modules:
  0.0 203.8 jit_solution(15071002989443741158)
XLA Ops:
  0.6 0.0 copy-start
  0.6 0.9 copy.28
  1.6 0.1 eq.59
  1.7 0.1 eq.55
  1.9 0.6 reduce-window.6
  2.5 0.2 slice_reduce_fusion
  2.7 0.1 fusion.29
  2.8 0.1 reduce_sum.41
  3.0 0.1 copy.30
  3.0 0.7 multiply_add_fusion
  3.7 1.2 convert_reduce_fusion
  4.9 1.3 fusion.6
  6.3 2.9 %convolution_convert_fusion = bf16[384,2048]{1,0:T(8,128)(2,1)} fusion(s32[128]{0:T(128)S(1)} %get-tuple-element.9, s32[128]{0:T(128)S(1)} %get-tuple-element.8, bf16[128,2048]{1,0:T(8,128)(2,1)} %param.26, f32[2048]{0:T(1024)} %param.27, f32[128]{0:T(128)S(1)} %add_rsqrt_fusion, f32[128]{0:T(128)S(1)} %broadcast_multiply_fusion), kind=kOutput, calls=%fused_computation | convolution fusion | flops 203571200 | bytes 2107392 | tf_op jit(solution)/shard_map/dot_general | solution.py:465
  9.2 5.3 %all-to-all-start = ((bf16[4,96,2048]{2,1,0:T(8,128)(2,1)}), bf16[4,96,2048]{2,1,0:T(8,128)(2,1)}, u32[]{:S(2)}, u32[]{:S(2)}) async-start(bf16[4,96,2048]{2,1,0:T(8,128)(2,1)} %bitcast.35), calls=%async_computation | async-start | bytes 3145728 | tf_op jit(solution)/shard_map/all_to_all | solution.py:469
  14.6 0.0 copy-done.6
  14.6 0.0 copy-done.3
  14.6 0.0 copy-done.4
  14.6 2.8 %pad_maximum_fusion.weight_ref = bf16[8,64,2048]{2,1,0:T(8,128)(2,1)} fusion(bf16[2,64,2048]{2,1,0:T(8,128)(2,1)S(1)} %bitcast.36, bf16[2,64,2048]{2,1,0:T(8,128)(2,1)S(1)} %bitcast.37, bf16[2,64,2048]{2,1,0:T(8,128)(2,1)} %bitcast.38, bf16[2,64,2048]{2,1,0:T(8,128)(2,1)} %bitcast.39), kind=kLoop, calls=%fused_computation.4 | loop fusion | flops 3145728 | bytes 4194304 | tf_op jit(solution)/shard_map/concatenate | solution.py:533
  17.4 148.9 %shard_map.185 = (bf16[128,1024]{1,0:T(8,128)(2,1)}, bf16[4096,2048]{1,0:T(8,128)(2,1)}) custom-call(bf16[1024,128]{1,0:T(8,128)(2,1)} %r_ref.1, bf16[1024,128]{1,0:T(8,128)(2,1)} %k_ref.1, bf16[1024,128]{1,0:T(8,128)(2,1)} %v_ref.1, bf16[1024,128]{1,0:T(8,128)(2,1)} %d_ref.1, bf16[1024,128]{1,0:T(8,128)(2,1)} %b_ref.1, bf16[1024,128]{1,0:T(8,128)(2,1)} %gate_ref.1, ...), custom_call_target="tpu_custom_call" | custom-call | flops 6710886400 | bytes 33554432 | tf_op jit(solution)/shard_map/pallas_call | solution.py:376
  166.3 0.0 all-to-all-done
  166.4 8.2 %shard_map.187 = bf16[4,2,48,2048]{3,2,1,0:T(8,128)(2,1)} custom-call(bf16[4,2,48,2048]{3,2,1,0:T(8,128)(2,1)} %bitcast.12.x_ref, bf16[8,512,2048]{2,1,0:T(8,128)(2,1)} %bitcast.31, bf16[8,512,2048]{2,1,0:T(8,128)(2,1)} %bitcast.32, bf16[8,512,2048]{2,1,0:T(8,128)(2,1)} %bitcast.33), custom_call_target="tpu_custom_call" | custom-call | flops 2415919104 | bytes 16777216 | tf_op jit(solution)/shard_map/pallas_call | solution.py:478
  174.5 4.3 %all-to-all-start.1 = ((bf16[4,96,2048]{2,1,0:T(8,128)(2,1)}), bf16[4,96,2048]{2,1,0:T(8,128)(2,1)}, u32[]{:S(2)}, u32[]{:S(2)}) async-start(bf16[4,96,2048]{2,1,0:T(8,128)(2,1)} %bitcast.34), calls=%async_computation.1 | async-start | bytes 3145728 | tf_op jit(solution)/shard_map/all_to_all | solution.py:493
  178.9 0.0 copy-start.1
  178.9 0.0 copy-start.5
  178.9 3.5 %shard_map.186 = bf16[128,2048]{1,0:T(8,128)(2,1)} custom-call(bf16[128,1024]{1,0:T(8,128)(2,1)} %get-tuple-element.4.rows_ref, bf16[4096,2048]{1,0:T(8,128)(2,1)} %get-tuple-element.5.weight_ref), custom_call_target="tpu_custom_call" | custom-call | flops 536870912 | bytes 5242880 | tf_op jit(solution)/shard_map/pallas_call | solution.py:541
  182.4 0.0 copy-done.1
  182.4 0.0 copy-done.5
  182.4 2.1 %fusion.37 = f32[128,512]{1,0:T(8,128)S(1)} fusion(bf16[2048,512]{1,0:T(8,128)(2,1)} %param.33, bf16[128,2048]{1,0:T(8,128)(2,1)S(1)} %copy-done.1, f32[2048]{0:T(1024)S(1)} %copy-done.5, f32[128]{0:T(128)S(1)} %add_rsqrt_fusion, f32[128]{0:T(128)S(1)} %broadcast_multiply_fusion), kind=kOutput, calls=%fused_computation.53 | convolution fusion | flops 269746176 | bytes 2892800 | tf_op jit(solution)/shard_map/dot_general | solution.py:472
  184.5 3.4 %fusion.5 = f32[128,2048]{1,0:T(8,128)} fusion(bf16[512,2048]{1,0:T(8,128)(2,1)S(1)} %copy-done, bf16[2048,512]{1,0:T(8,128)(2,1)} %param.34, f32[128,512]{1,0:T(8,128)S(1)} %fusion.37, bf16[128,2048]{1,0:T(8,128)(2,1)S(1)} %copy-done.1, f32[2048]{0:T(1024)S(1)} %copy-done.5, f32[128]{0:T(128)S(1)} %add_rsqrt_fusion, f32[128]{0:T(128)S(1)} %broadcast_multiply_fusion), kind=kOutput, calls=%fused_computation.11 | convolution fusion | flops 538574848 | bytes 6038528 | tf_op jit(solution)/shard_map/dot_general | solution.py:475
  188.0 11.2 %all-to-all-done.1 = bf16[4,96,2048]{2,1,0:T(8,128)(2,1)} async-done(((bf16[4,96,2048]{2,1,0:T(8,128)(2,1)}), bf16[4,96,2048]{2,1,0:T(8,128)(2,1)}, u32[]{:S(2)}, u32[]{:S(2)}) %all-to-all-start.1) | async-done | bytes 1572896 | tf_op jit(solution)/shard_map/all_to_all | solution.py:493
  199.1 1.9 fusion.26
  201.1 2.7 %fusion.1 = bf16[128,2048]{1,0:T(8,128)(2,1)} fusion(f32[128,2048]{1,0:T(8,128)S(1)} %copy-done.2, f32[128,2048]{1,0:T(8,128)S(1)} %fusion.26, bf16[384,2048]{1,0:T(8,128)(2,1)} %bitcast.15, f32[128]{0:T(128)S(1)} %get-tuple-element.7, s32[128]{0:T(128)S(1)} %get-tuple-element.9, f32[128]{0:T(128)S(1)} %get-tuple-element.6, s32[128]{0:T(128)S(1)} %get-tuple-element.8), kind=kOutput, calls=%fused_computation.3 | convolution fusion | flops 202555392 | bytes 4196352 | tf_op jit(solution)/shard_map/dot_general | solution.py:500
  (15 shorter events, 0.1 us)
Async XLA Ops:
  0.6 183.9 %copy-start = (bf16[512,2048]{1,0:T(8,128)(2,1)S(1)}, bf16[512,2048]{1,0:T(8,128)(2,1)}, u32[]{:S(2)}) copy-start(bf16[512,2048]{1,0:T(8,128)(2,1)} %param.35) | copy-start | bytes 6291460
  9.2 5.3 %copy-start.6 = (f32[128,2]{0,1:T(2,128)S(1)}, f32[128,2]{0,1:T(2,128)}, u32[]{:S(2)}) copy-start(f32[128,2]{0,1:T(2,128)} %param.29) | copy-start | bytes 3076
  9.2 5.4 %copy-start.3 = (bf16[128,2048]{1,0:T(8,128)(2,1)S(1)}, bf16[128,2048]{1,0:T(8,128)(2,1)}, u32[]{:S(2)}) copy-start(bf16[128,2048]{1,0:T(8,128)(2,1)} %param.25) | copy-start | bytes 1572868
  9.2 5.4 %copy-start.4 = (bf16[2,2048,64]{1,2,0:T(8,128)(2,1)S(1)}, bf16[2,2048,64]{1,2,0:T(8,128)(2,1)}, u32[]{:S(2)}) copy-start(bf16[2,2048,64]{1,2,0:T(8,128)(2,1)} %param.32) | copy-start | bytes 1572868
  9.2 157.1 %all-to-all-start = ((bf16[4,96,2048]{2,1,0:T(8,128)(2,1)}), bf16[4,96,2048]{2,1,0:T(8,128)(2,1)}, u32[]{:S(2)}, u32[]{:S(2)}) async-start(bf16[4,96,2048]{2,1,0:T(8,128)(2,1)} %bitcast.35), calls=%async_computation | async-start | bytes 3145728 | tf_op jit(solution)/shard_map/all_to_all | solution.py:469
  174.5 24.6 %all-to-all-start.1 = ((bf16[4,96,2048]{2,1,0:T(8,128)(2,1)}), bf16[4,96,2048]{2,1,0:T(8,128)(2,1)}, u32[]{:S(2)}, u32[]{:S(2)}) async-start(bf16[4,96,2048]{2,1,0:T(8,128)(2,1)} %bitcast.34), calls=%async_computation.1 | async-start | bytes 3145728 | tf_op jit(solution)/shard_map/all_to_all | solution.py:493
  178.9 3.6 %copy-start.1 = (bf16[128,2048]{1,0:T(8,128)(2,1)S(1)}, bf16[128,2048]{1,0:T(8,128)(2,1)}, u32[]{:S(2)}) copy-start(bf16[128,2048]{1,0:T(8,128)(2,1)} %param.26) | copy-start | bytes 1572868
  178.9 3.6 %copy-start.5 = (f32[2048]{0:T(1024)S(1)}, f32[2048]{0:T(1024)}, u32[]{:S(2)}) copy-start(f32[2048]{0:T(1024)} %param.27) | copy-start | bytes 24580
  188.0 13.1 %copy-start.2 = (f32[128,2048]{1,0:T(8,128)S(1)}, f32[128,2048]{1,0:T(8,128)}, u32[]{:S(2)}) copy-start(f32[128,2048]{1,0:T(8,128)} %fusion.5) | copy-start | bytes 3145732

commit v3 on v2

--- a/solution.py
+++ b/solution.py
@@ -133,8 +133,10 @@
     gate_ref,
     gain_ref,
     weight_ref,
+    slab_ref,
     token_ref,
     whole_ref,
+    project_ref,
     state,
     qp_ref,
     lo_ref,
@@ -149,6 +151,10 @@
     row_send,
     row_recv,
     own_sem,
+    slab_ring_send,
+    slab_ring_recv,
+    slab_send,
+    slab_recv,
 ):
     two = 2 * BLOCK
     peers = 2 * ring
@@ -164,10 +170,7 @@
     MESH = pl.DeviceIdType.MESH
 
     def place(chunk, origin):
-        last = chunk // (chunks - 2)
-        base = (1 - last) * (chunk * span + origin * height) + last * (
-            (chunks - 2) * span + origin * 2 * height + (chunk - chunks + 2) * height
-        )
+        base = chunk * span + origin * height
         return whole_ref.at[pl.ds(pl.multiple_of(base, height), height), :]
 
     def ring_copy(source, chunk, origin, step, target):
@@ -190,6 +193,62 @@
             device_id_type=MESH,
         )
 
+    half, columns = slab_ref.shape[0] // 2, slab_ref.shape[1]
+
+    def slab_place(way, origin):
+        return project_ref.at[
+            pl.ds(pl.multiple_of(origin * 2 * half + way * half, half), half),
+            pl.ds(pl.multiple_of(here * columns, columns), columns),
+        ]
+
+    def slab_ring(source, way, origin, step):
+        return pltpu.make_async_remote_copy(
+            src_ref=source,
+            dst_ref=slab_place(way, origin),
+            send_sem=slab_ring_send.at[way, step],
+            recv_sem=slab_ring_recv.at[way, step],
+            device_id={"tp": (after, before)[way]},
+            device_id_type=MESH,
+        )
+
+    def slab_copies(source, way, origin, step):
+        for q in range(groups):
+            for flip in (0, 1):
+                if q or flip:
+                    yield pltpu.make_async_remote_copy(
+                        src_ref=source,
+                        dst_ref=slab_place(way, origin),
+                        send_sem=slab_send.at[way, step, q, flip],
+                        recv_sem=slab_recv.at[way, step, q, flip],
+                        device_id={
+                            "ep": (here + q) % groups,
+                            "tp": (mine, partner)[flip],
+                        },
+                        device_id_type=MESH,
+                    )
+
+    def slab_own(way):
+        return pltpu.make_async_copy(
+            slab_ref.at[pl.ds(way * half, half), :],
+            slab_place(way, mine),
+            own_sem.at[chunks + 1 + way],
+        )
+
+    def slab_relay(hop, carry):
+        for way in (0, 1):
+            shift = ring - hop if way == 0 else hop
+            origin = (depth + shift) % ring * 2 + core
+            block = slab_place(way, origin)
+            slab_ring(block, way, origin, hop - 1).wait_recv()
+
+            @pl.when(hop < ring - 1)
+            def _():
+                slab_ring(block, way, origin, hop).start()
+
+            for copy in slab_copies(block, way, origin, hop):
+                copy.start()
+        return carry
+
     def own_copy(chunk):
         return pltpu.make_async_copy(
             weight_ref.at[chunk], place(chunk, mine), own_sem.at[chunk]
@@ -204,7 +263,20 @@
         pl.semaphore_signal(
             barrier, inc=1, device_id={"ep": (here + q) % groups}, device_id_type=MESH
         )
-    pl.semaphore_wait(barrier, peers + groups - 2)
+    for q in range(1, groups):
+        pl.semaphore_signal(
+            barrier,
+            inc=1,
+            device_id={"ep": (here + q) % groups, "tp": partner},
+            device_id_type=MESH,
+        )
+    pl.semaphore_wait(barrier, peers + 2 * groups - 3)
+    for way in (0, 1):
+        piece = slab_ref.at[pl.ds(way * half, half), :]
+        slab_ring(piece, way, mine, 0).start()
+        slab_own(way).start()
+        for copy in slab_copies(piece, way, mine, 0):
+            copy.start()
 
     def begin(kind, carry):
         for way, target in ((0, after), (1, before)):
@@ -260,6 +332,10 @@
             now = jnp.concatenate([moved[:two], moved[two:] + maps[two:]], axis=0)
         state[...] = now
 
+        @pl.when((step >= 1) & (step < ring))
+        def _():
+            slab_relay(step, 0)
+
         @pl.when(step < inside)
         def _():
             lax.fori_loop(step * each, (step + 1) * each, relay, 0)
@@ -332,7 +408,24 @@
 
     lax.fori_loop(1, peers, row_start, 0)
 
+    lax.fori_loop(min(turns, ring), ring, slab_relay, 0)
     lax.fori_loop(inside * each, relays, relay, 0)
+
+    def slab_close(hop, carry):
+        for way in (0, 1):
+            piece = slab_ref.at[pl.ds(way * half, half), :]
+            for copy in slab_copies(piece, way, mine, hop):
+                copy.wait()
+
+            @pl.when(hop < ring - 1)
+            def _():
+                slab_ring(piece, way, mine, hop).wait_send()
+
+        return carry
+
+    lax.fori_loop(0, ring, slab_close, 0)
+    slab_own(0).wait()
+    slab_own(1).wait()
 
     def close(chunk, carry):
         own_copy(chunk).wait()
@@ -362,7 +455,7 @@
 
 
 def mixer_and_weights(
-    receptance, key_in, payload_vectors, decay_in, rate_in, gate_in, norm_gain, weights
+    receptance, key_in, payload_vectors, decay_in, rate_in, gate_in, norm_gain, weights, out_weight
 ):
     length, channels = receptance.shape
     groups, peers = lax.axis_size("ep"), lax.axis_size("tp")
@@ -373,14 +466,17 @@
     chunks, height, width = weights.shape
     vmem = pl.BlockSpec(memory_space=pltpu.VMEM)
     dma = pltpu.SemaphoreType.DMA
-    tokens, whole = pl.pallas_call(
+    columns = width // groups
+    slab = lax.dynamic_slice_in_dim(out_weight, lax.axis_index("ep") * columns, columns, axis=1)
+    tokens, whole, project = pl.pallas_call(
         functools.partial(mixer_kernel, 4, groups, ring),
         out_shape=(
             jax.ShapeDtypeStruct((length // peers, peers * wide), jnp.bfloat16),
             jax.ShapeDtypeStruct((chunks * peers * height, width), jnp.bfloat16),
+            jax.ShapeDtypeStruct((peers * out_weight.shape[0], width), jnp.bfloat16),
         ),
-        in_specs=[vmem] * 8,
-        out_specs=(vmem, pl.BlockSpec(memory_space=pl.ANY)),
+        in_specs=[vmem] * 9,
+        out_specs=(vmem, pl.BlockSpec(memory_space=pl.ANY), pl.BlockSpec(memory_space=pl.ANY)),
         scratch_shapes=[
             pltpu.VMEM((2 * wide, wide), jnp.float32),
             pltpu.VMEM((length, wide), jnp.float32),
@@ -395,7 +491,11 @@
             dma((groups,)),
             dma((peers,)),
             dma((peers,)),
-            dma((chunks + 1,)),
+            dma((chunks + 3,)),
+            dma((2, ring)),
+            dma((2, ring)),
+            dma((2, ring, groups, 2)),
+            dma((2, ring, groups, 2)),
         ],
         compiler_params=pltpu.CompilerParams(collective_id=0, has_side_effects=True),
         cost_estimate=pl.CostEstimate(
@@ -410,10 +510,11 @@
         pad(gate_in),
         pad(norm_gain).reshape(1, wide),
         weights,
+        slab,
     )
     if spare:
         tokens = tokens.reshape(-1, peers, wide)[:, :, :channels].reshape(-1, peers * channels)
-    return tokens, whole
+    return tokens, whole, project
 
 
 def silu(x):
@@ -531,12 +632,18 @@
 ):
     local_count, width, part = expert_gate.shape
     weights = jnp.concatenate(
-        [jnp.swapaxes(w, 1, 2) for w in (expert_gate, expert_up, expert_down)]
-        + [out_weight.reshape(2, part, width)],
-        axis=0,
-    )
-    token_rows, whole = mixer_and_weights(
-        receptance, key_in, payload_vectors, decay_in, rate_in, gate_in, norm_gain, weights
+        [jnp.swapaxes(w, 1, 2) for w in (expert_gate, expert_up, expert_down)], axis=0
+    )
+    token_rows, whole, project = mixer_and_weights(
+        receptance,
+        key_in,
+        payload_vectors,
+        decay_in,
+        rate_in,
+        gate_in,
+        norm_gain,
+        weights,
+        out_weight,
     )
     mixed = pl.pallas_call(
         project_kernel,
@@ -544,20 +651,20 @@
         out_shape=jax.ShapeDtypeStruct((token_rows.shape[0], width), jnp.bfloat16),
         in_specs=[
             pl.BlockSpec(token_rows.shape, lambda n: (0, 0)),
-            pl.BlockSpec((token_rows.shape[1], width // 2), lambda n: (3, n)),
+            pl.BlockSpec((token_rows.shape[1], width // 2), lambda n: (0, n)),
         ],
         out_specs=pl.BlockSpec((token_rows.shape[0], width // 2), lambda n: (0, n)),
         cost_estimate=pl.CostEstimate(
             flops=2 * token_rows.size * width, bytes_accessed=5 << 20, transcendentals=0
         ),
-    )(token_rows, whole)
+    )(token_rows, project)
     moe_out = expert_layer(
         moe_in,
         moe_gain,
         routes,
         route_weights,
         local_count,
-        whole.reshape(4 * local_count, -1, width),
+        whole.reshape(3 * local_count, -1, width),
         shared_gate,
         shared_up,
         shared_down,

time: 204 us -> 181 us (0.89)
  Pallas kernels: 161 us -> 136 us
    pallas_call x1, Pallas kernels: 149 us -> 125 us  [mixer_and_weights(): pl.pallas_call(functools.partial(mixer_kernel, 4, groups, ring), out_shap...]
  transfers between devices with their start and end apart: 2 -> 2, of which waited for: 1 -> 1; matrix products, arithmetic and copies ran while one was open for 4% -> 5% of each run, Pallas kernels for 75% -> 71%
where the time goes in v3:
time: 181 us; the launch traced here: 180 us
  Pallas kernels  136 us (75%)
  matrix products  12.8 us (7%)
  waiting for transfers between devices  11.1 us (6%)
  starting transfers between devices  9.66 us (5%)
  other arithmetic  6.5 us (4%)
  local copies, waits for them, and re-layouts  3.25 us (2%)
    pallas_call x1, Pallas kernels, mixer_and_weights(): pl.pallas_call(functools.partial(mixer_kernel, 4, groups, ring), out_shap...  125 us
    all_to_all x1, waiting for transfers between devices, expert_layer(): lax.all_to_all(sending, 'ep', split_axis=0, concat_axis=0, tiled=True)  11.1 us
    pallas_call x1, Pallas kernels, expert_layer(): pl.pallas_call(ffn_kernel, grid=(local_count,), out_shape=jax.ShapeDtypeS...  8.14 us
    all_to_all x1, starting transfers between devices, expert_layer(): lax.all_to_all(outgoing, 'ep', split_axis=0, concat_axis=0, tiled=True)  5.32 us
    all_to_all x1, starting transfers between devices, expert_layer(): lax.all_to_all(sending, 'ep', split_axis=0, concat_axis=0, tiled=True)  4.34 us
  transfers between devices with their start and end apart: 2, of which 1 were waited for; matrix products, arithmetic and copies ran while one was open for 5% of the time, Pallas kernels for 71%

profile of v3, /device:TPU:0, one launch (start us, length us, event | category | flops | bytes accessed | tf_op | source)
XLA Modules:
  0.0 180.2 jit_solution(13689036814063547377)
XLA Ops:
  0.6 0.0 copy-start
  0.6 0.0 copy-start.1
  0.7 0.9 copy.28
  1.6 0.1 eq.59
  1.7 0.1 eq.55
  1.9 1.2 convert_reduce_fusion
  3.1 1.3 fusion.6
  4.4 0.6 reduce-window.6
  5.0 0.2 slice_reduce_fusion
  5.3 0.1 fusion.29
  5.4 0.1 reduce_sum.41
  5.5 0.1 copy.30
  5.6 0.7 multiply_add_fusion
  6.3 0.0 copy-done.1
  6.3 2.6 %convolution_convert_fusion = bf16[384,2048]{1,0:T(8,128)(2,1)} fusion(s32[128]{0:T(128)S(1)} %get-tuple-element.11, s32[128]{0:T(128)S(1)} %get-tuple-element.10, bf16[128,2048]{1,0:T(8,128)(2,1)S(1)} %copy-done.1, f32[2048]{0:T(1024)} %param.27, f32[128]{0:T(128)S(1)} %add_rsqrt_fusion, f32[128]{0:T(128)S(1)} %broadcast_multiply_fusion), kind=kOutput, calls=%fused_computation | convolution fusion | flops 203571200 | bytes 2107392 | tf_op jit(solution)/shard_map/dot_general | solution.py:566
  8.9 5.3 %all-to-all-start = ((bf16[4,96,2048]{2,1,0:T(8,128)(2,1)}), bf16[4,96,2048]{2,1,0:T(8,128)(2,1)}, u32[]{:S(2)}, u32[]{:S(2)}) async-start(bf16[4,96,2048]{2,1,0:T(8,128)(2,1)} %bitcast.34), calls=%async_computation | async-start | bytes 3145728 | tf_op jit(solution)/shard_map/all_to_all | solution.py:570
  14.2 0.0 copy-done.5
  14.2 1.6 constant_dynamic-slice_fusion.slab_ref
  15.8 2.5 %pad_maximum_fusion.weight_ref = bf16[6,64,2048]{2,1,0:T(8,128)(2,1)} fusion(bf16[2,64,2048]{2,1,0:T(8,128)(2,1)S(1)} %bitcast.35, bf16[2,64,2048]{2,1,0:T(8,128)(2,1)} %bitcast.36, bf16[2,64,2048]{2,1,0:T(8,128)(2,1)} %bitcast.37), kind=kLoop, calls=%fused_computation.4 | loop fusion | flops 1572864 | bytes 3145728 | tf_op jit(solution)/shard_map/concatenate | solution.py:634
  18.3 124.5 %shard_map.185 = (bf16[128,1024]{1,0:T(8,128)(2,1)}, bf16[3072,2048]{1,0:T(8,128)(2,1)}, bf16[1024,2048]{1,0:T(8,128)(2,1)}) custom-call(bf16[1024,128]{1,0:T(8,128)(2,1)} %r_ref.1, bf16[1024,128]{1,0:T(8,128)(2,1)} %k_ref.1, bf16[1024,128]{1,0:T(8,128)(2,1)} %v_ref.1, bf16[1024,128]{1,0:T(8,128)(2,1)} %d_ref.1, bf16[1024,128]{1,0:T(8,128)(2,1)} %b_ref.1, ...), custom_call_target="tpu_custom_call" | custom-call | flops 6710886400 | bytes 33554432 | tf_op jit(solution)/shard_map/pallas_call | solution.py:471
  142.8 0.0 all-to-all-done
  142.8 8.1 %shard_map.187 = bf16[4,2,48,2048]{3,2,1,0:T(8,128)(2,1)} custom-call(bf16[4,2,48,2048]{3,2,1,0:T(8,128)(2,1)} %bitcast.11.x_ref, bf16[6,512,2048]{2,1,0:T(8,128)(2,1)} %bitcast.30, bf16[6,512,2048]{2,1,0:T(8,128)(2,1)} %bitcast.31, bf16[6,512,2048]{2,1,0:T(8,128)(2,1)} %bitcast.32), custom_call_target="tpu_custom_call" | custom-call | flops 2415919104 | bytes 16777216 | tf_op jit(solution)/shard_map/pallas_call | solution.py:579
  151.0 4.3 %all-to-all-start.1 = ((bf16[4,96,2048]{2,1,0:T(8,128)(2,1)}), bf16[4,96,2048]{2,1,0:T(8,128)(2,1)}, u32[]{:S(2)}, u32[]{:S(2)}) async-start(bf16[4,96,2048]{2,1,0:T(8,128)(2,1)} %bitcast.33), calls=%async_computation.1 | async-start | bytes 3145728 | tf_op jit(solution)/shard_map/all_to_all | solution.py:594
  155.3 0.0 copy-start.4
  155.3 3.5 %shard_map.186 = bf16[128,2048]{1,0:T(8,128)(2,1)} custom-call(bf16[128,1024]{1,0:T(8,128)(2,1)} %get-tuple-element.5.rows_ref, bf16[1024,2048]{1,0:T(8,128)(2,1)} %get-tuple-element.6.weight_ref), custom_call_target="tpu_custom_call" | custom-call | flops 536870912 | bytes 5242880 | tf_op jit(solution)/shard_map/pallas_call | solution.py:648
  158.8 0.0 copy-done.4
  158.8 2.1 %fusion.37 = f32[128,512]{1,0:T(8,128)S(1)} fusion(bf16[2048,512]{1,0:T(8,128)(2,1)} %param.33, bf16[128,2048]{1,0:T(8,128)(2,1)S(1)} %copy-done.1, f32[2048]{0:T(1024)S(1)} %copy-done.4, f32[128]{0:T(128)S(1)} %add_rsqrt_fusion, f32[128]{0:T(128)S(1)} %broadcast_multiply_fusion), kind=kOutput, calls=%fused_computation.54 | convolution fusion | flops 269746176 | bytes 2892800 | tf_op jit(solution)/shard_map/dot_general | solution.py:573
  160.9 3.5 %fusion.5 = f32[128,2048]{1,0:T(8,128)} fusion(bf16[512,2048]{1,0:T(8,128)(2,1)S(1)} %copy-done, bf16[2048,512]{1,0:T(8,128)(2,1)} %param.34, f32[128,512]{1,0:T(8,128)S(1)} %fusion.37, bf16[128,2048]{1,0:T(8,128)(2,1)S(1)} %copy-done.1, f32[2048]{0:T(1024)S(1)} %copy-done.4, f32[128]{0:T(128)S(1)} %add_rsqrt_fusion, f32[128]{0:T(128)S(1)} %broadcast_multiply_fusion), kind=kOutput, calls=%fused_computation.11 | convolution fusion | flops 538574848 | bytes 6038528 | tf_op jit(solution)/shard_map/dot_general | solution.py:576
  164.4 11.1 %all-to-all-done.1 = bf16[4,96,2048]{2,1,0:T(8,128)(2,1)} async-done(((bf16[4,96,2048]{2,1,0:T(8,128)(2,1)}), bf16[4,96,2048]{2,1,0:T(8,128)(2,1)}, u32[]{:S(2)}, u32[]{:S(2)}) %all-to-all-start.1) | async-done | bytes 1572896 | tf_op jit(solution)/shard_map/all_to_all | solution.py:594
  175.5 2.0 %fusion.26 = f32[128,2048]{1,0:T(8,128)S(1)} fusion(bf16[384,2048]{1,0:T(8,128)(2,1)} %bitcast.14, f32[128]{0:T(128)S(1)} %get-tuple-element.9, s32[128]{0:T(128)S(1)} %get-tuple-element.11, f32[128]{0:T(128)S(1)} %get-tuple-element.8, s32[128]{0:T(128)S(1)} %get-tuple-element.10), kind=kOutput, calls=%fused_computation.34 | convolution fusion | flops 201621504 | bytes 2623488 | tf_op jit(solution)/shard_map/dot_general | solution.py:601
  177.5 0.0 copy-done.2
  177.5 2.7 %fusion.1 = bf16[128,2048]{1,0:T(8,128)(2,1)} fusion(f32[128,2048]{1,0:T(8,128)S(1)} %copy-done.2, f32[128,2048]{1,0:T(8,128)S(1)} %fusion.26, bf16[384,2048]{1,0:T(8,128)(2,1)} %bitcast.14, f32[128]{0:T(128)S(1)} %get-tuple-element.9, s32[128]{0:T(128)S(1)} %get-tuple-element.11, f32[128]{0:T(128)S(1)} %get-tuple-element.8, s32[128]{0:T(128)S(1)} %get-tuple-element.10), kind=kOutput, calls=%fused_computation.3 | convolution fusion | flops 202555392 | bytes 4196352 | tf_op jit(solution)/shard_map/dot_general | solution.py:601
  (14 shorter events, 0.1 us)
Async XLA Ops:
  0.6 160.3 %copy-start = (bf16[512,2048]{1,0:T(8,128)(2,1)S(1)}, bf16[512,2048]{1,0:T(8,128)(2,1)}, u32[]{:S(2)}) copy-start(bf16[512,2048]{1,0:T(8,128)(2,1)} %param.35) | copy-start | bytes 6291460
  0.6 5.7 %copy-start.1 = (bf16[128,2048]{1,0:T(8,128)(2,1)S(1)}, bf16[128,2048]{1,0:T(8,128)(2,1)}, u32[]{:S(2)}) copy-start(bf16[128,2048]{1,0:T(8,128)(2,1)} %param.26) | copy-start | bytes 1572868
  8.9 5.3 %copy-start.5 = (f32[128,2]{0,1:T(2,128)S(1)}, f32[128,2]{0,1:T(2,128)}, u32[]{:S(2)}) copy-start(f32[128,2]{0,1:T(2,128)} %param.29) | copy-start | bytes 3076
  8.9 6.9 %copy-start.3 = (bf16[2,2048,64]{1,2,0:T(8,128)(2,1)S(1)}, bf16[2,2048,64]{1,2,0:T(8,128)(2,1)}, u32[]{:S(2)}) copy-start(bf16[2,2048,64]{1,2,0:T(8,128)(2,1)} %param.32) | copy-start | bytes 1572868
  8.9 134.0 %all-to-all-start = ((bf16[4,96,2048]{2,1,0:T(8,128)(2,1)}), bf16[4,96,2048]{2,1,0:T(8,128)(2,1)}, u32[]{:S(2)}, u32[]{:S(2)}) async-start(bf16[4,96,2048]{2,1,0:T(8,128)(2,1)} %bitcast.34), calls=%async_computation | async-start | bytes 3145728 | tf_op jit(solution)/shard_map/all_to_all | solution.py:570
  151.0 24.5 %all-to-all-start.1 = ((bf16[4,96,2048]{2,1,0:T(8,128)(2,1)}), bf16[4,96,2048]{2,1,0:T(8,128)(2,1)}, u32[]{:S(2)}, u32[]{:S(2)}) async-start(bf16[4,96,2048]{2,1,0:T(8,128)(2,1)} %bitcast.33), calls=%async_computation.1 | async-start | bytes 3145728 | tf_op jit(solution)/shard_map/all_to_all | solution.py:594
  155.3 3.5 %copy-start.4 = (f32[2048]{0:T(1024)S(1)}, f32[2048]{0:T(1024)}, u32[]{:S(2)}) copy-start(f32[2048]{0:T(1024)} %param.27) | copy-start | bytes 24580
  175.5 2.0 %copy-start.2 = (f32[128,2048]{1,0:T(8,128)S(1)}, f32[128,2048]{1,0:T(8,128)}, u32[]{:S(2)}) copy-start(f32[128,2048]{1,0:T(8,128)} %fusion.5) | copy-start | bytes 3145732

commit v4 on v3

--- a/solution.py
+++ b/solution.py
@@ -309,7 +309,7 @@
     state[...] = jnp.where(row == col, 1.0, 0.0)
     turns = r_ref.shape[0] // (BLOCK * unroll)
     relays = (ring - 1) * kinds
-    each = 2
+    each = 1
     inside = min(turns, relays // each)
 
     def turn(step, carry):

time: 181 us -> 183 us (1.011)
  Pallas kernels: 136 us -> 138 us
    pallas_call x1, Pallas kernels: 125 us -> 126 us  [mixer_and_weights(): pl.pallas_call(functools.partial(mixer_kernel, 4, groups, ring), out_shap...]
where the time goes in v4:
time: 183 us; the launch traced here: 182 us
  Pallas kernels  138 us (75%)
  matrix products  12.8 us (7%)
  waiting for transfers between devices  11 us (6%)
  starting transfers between devices  9.66 us (5%)
  other arithmetic  6.5 us (4%)
  local copies, waits for them, and re-layouts  3.25 us (2%)
    pallas_call x1, Pallas kernels, mixer_and_weights(): pl.pallas_call(functools.partial(mixer_kernel, 4, groups, ring), out_shap...  126 us
    all_to_all x1, waiting for transfers between devices, expert_layer(): lax.all_to_all(sending, 'ep', split_axis=0, concat_axis=0, tiled=True)  11 us
    pallas_call x1, Pallas kernels, expert_layer(): pl.pallas_call(ffn_kernel, grid=(local_count,), out_shape=jax.ShapeDtypeS...  8.14 us
    all_to_all x1, starting transfers between devices, expert_layer(): lax.all_to_all(outgoing, 'ep', split_axis=0, concat_axis=0, tiled=True)  5.32 us
    all_to_all x1, starting transfers between devices, expert_layer(): lax.all_to_all(sending, 'ep', split_axis=0, concat_axis=0, tiled=True)  4.34 us
  transfers between devices with their start and end apart: 2, of which 1 were waited for; matrix products, arithmetic and copies ran while one was open for 5% of the time, Pallas kernels for 71%

profile of v4, /device:TPU:0, one launch (start us, length us, event | category | flops | bytes accessed | tf_op | source)
XLA Modules:
  0.0 182.2 jit_solution(14587807348004375546)
XLA Ops:
  0.6 0.0 copy-start
  0.6 0.0 copy-start.1
  0.7 0.9 copy.28
  1.6 0.1 eq.59
  1.7 0.1 eq.55
  1.9 1.2 convert_reduce_fusion
  3.1 1.3 fusion.6
  4.4 0.6 reduce-window.6
  5.0 0.2 slice_reduce_fusion
  5.3 0.1 fusion.29
  5.4 0.1 reduce_sum.41
  5.5 0.1 copy.30
  5.6 0.7 multiply_add_fusion
  6.3 0.0 copy-done.1
  6.3 2.6 %convolution_convert_fusion = bf16[384,2048]{1,0:T(8,128)(2,1)} fusion(s32[128]{0:T(128)S(1)} %get-tuple-element.11, s32[128]{0:T(128)S(1)} %get-tuple-element.10, bf16[128,2048]{1,0:T(8,128)(2,1)S(1)} %copy-done.1, f32[2048]{0:T(1024)} %param.27, f32[128]{0:T(128)S(1)} %add_rsqrt_fusion, f32[128]{0:T(128)S(1)} %broadcast_multiply_fusion), kind=kOutput, calls=%fused_computation | convolution fusion | flops 203571200 | bytes 2107392 | tf_op jit(solution)/shard_map/dot_general | solution.py:566
  8.9 5.3 %all-to-all-start = ((bf16[4,96,2048]{2,1,0:T(8,128)(2,1)}), bf16[4,96,2048]{2,1,0:T(8,128)(2,1)}, u32[]{:S(2)}, u32[]{:S(2)}) async-start(bf16[4,96,2048]{2,1,0:T(8,128)(2,1)} %bitcast.34), calls=%async_computation | async-start | bytes 3145728 | tf_op jit(solution)/shard_map/all_to_all | solution.py:570
  14.2 0.0 copy-done.5
  14.2 1.6 constant_dynamic-slice_fusion.slab_ref
  15.8 0.0 copy-done.3
  15.8 2.5 %pad_maximum_fusion.weight_ref = bf16[6,64,2048]{2,1,0:T(8,128)(2,1)} fusion(bf16[2,64,2048]{2,1,0:T(8,128)(2,1)S(1)} %bitcast.35, bf16[2,64,2048]{2,1,0:T(8,128)(2,1)} %bitcast.36, bf16[2,64,2048]{2,1,0:T(8,128)(2,1)} %bitcast.37), kind=kLoop, calls=%fused_computation.4 | loop fusion | flops 1572864 | bytes 3145728 | tf_op jit(solution)/shard_map/concatenate | solution.py:634
  18.3 126.5 %shard_map.185 = (bf16[128,1024]{1,0:T(8,128)(2,1)}, bf16[3072,2048]{1,0:T(8,128)(2,1)}, bf16[1024,2048]{1,0:T(8,128)(2,1)}) custom-call(bf16[1024,128]{1,0:T(8,128)(2,1)} %r_ref.1, bf16[1024,128]{1,0:T(8,128)(2,1)} %k_ref.1, bf16[1024,128]{1,0:T(8,128)(2,1)} %v_ref.1, bf16[1024,128]{1,0:T(8,128)(2,1)} %d_ref.1, bf16[1024,128]{1,0:T(8,128)(2,1)} %b_ref.1, ...), custom_call_target="tpu_custom_call" | custom-call | flops 6710886400 | bytes 33554432 | tf_op jit(solution)/shard_map/pallas_call | solution.py:471
  144.8 0.0 all-to-all-done
  144.8 8.1 %shard_map.187 = bf16[4,2,48,2048]{3,2,1,0:T(8,128)(2,1)} custom-call(bf16[4,2,48,2048]{3,2,1,0:T(8,128)(2,1)} %bitcast.11.x_ref, bf16[6,512,2048]{2,1,0:T(8,128)(2,1)} %bitcast.30, bf16[6,512,2048]{2,1,0:T(8,128)(2,1)} %bitcast.31, bf16[6,512,2048]{2,1,0:T(8,128)(2,1)} %bitcast.32), custom_call_target="tpu_custom_call" | custom-call | flops 2415919104 | bytes 16777216 | tf_op jit(solution)/shard_map/pallas_call | solution.py:579
  152.9 4.3 %all-to-all-start.1 = ((bf16[4,96,2048]{2,1,0:T(8,128)(2,1)}), bf16[4,96,2048]{2,1,0:T(8,128)(2,1)}, u32[]{:S(2)}, u32[]{:S(2)}) async-start(bf16[4,96,2048]{2,1,0:T(8,128)(2,1)} %bitcast.33), calls=%async_computation.1 | async-start | bytes 3145728 | tf_op jit(solution)/shard_map/all_to_all | solution.py:594
  157.3 0.0 copy-start.4
  157.3 3.5 %shard_map.186 = bf16[128,2048]{1,0:T(8,128)(2,1)} custom-call(bf16[128,1024]{1,0:T(8,128)(2,1)} %get-tuple-element.5.rows_ref, bf16[1024,2048]{1,0:T(8,128)(2,1)} %get-tuple-element.6.weight_ref), custom_call_target="tpu_custom_call" | custom-call | flops 536870912 | bytes 5242880 | tf_op jit(solution)/shard_map/pallas_call | solution.py:648
  160.8 2.1 %fusion.37 = f32[128,512]{1,0:T(8,128)S(1)} fusion(bf16[2048,512]{1,0:T(8,128)(2,1)} %param.33, bf16[128,2048]{1,0:T(8,128)(2,1)S(1)} %copy-done.1, f32[2048]{0:T(1024)S(1)} %copy-done.4, f32[128]{0:T(128)S(1)} %add_rsqrt_fusion, f32[128]{0:T(128)S(1)} %broadcast_multiply_fusion), kind=kOutput, calls=%fused_computation.54 | convolution fusion | flops 269746176 | bytes 2892800 | tf_op jit(solution)/shard_map/dot_general | solution.py:573
  162.9 0.0 copy-done
  162.9 3.5 %fusion.5 = f32[128,2048]{1,0:T(8,128)} fusion(bf16[512,2048]{1,0:T(8,128)(2,1)S(1)} %copy-done, bf16[2048,512]{1,0:T(8,128)(2,1)} %param.34, f32[128,512]{1,0:T(8,128)S(1)} %fusion.37, bf16[128,2048]{1,0:T(8,128)(2,1)S(1)} %copy-done.1, f32[2048]{0:T(1024)S(1)} %copy-done.4, f32[128]{0:T(128)S(1)} %add_rsqrt_fusion, f32[128]{0:T(128)S(1)} %broadcast_multiply_fusion), kind=kOutput, calls=%fused_computation.11 | convolution fusion | flops 538574848 | bytes 6038528 | tf_op jit(solution)/shard_map/dot_general | solution.py:576
  166.4 11.0 %all-to-all-done.1 = bf16[4,96,2048]{2,1,0:T(8,128)(2,1)} async-done(((bf16[4,96,2048]{2,1,0:T(8,128)(2,1)}), bf16[4,96,2048]{2,1,0:T(8,128)(2,1)}, u32[]{:S(2)}, u32[]{:S(2)}) %all-to-all-start.1) | async-done | bytes 1572896 | tf_op jit(solution)/shard_map/all_to_all | solution.py:594
  177.4 2.0 %fusion.26 = f32[128,2048]{1,0:T(8,128)S(1)} fusion(bf16[384,2048]{1,0:T(8,128)(2,1)} %bitcast.14, f32[128]{0:T(128)S(1)} %get-tuple-element.9, s32[128]{0:T(128)S(1)} %get-tuple-element.11, f32[128]{0:T(128)S(1)} %get-tuple-element.8, s32[128]{0:T(128)S(1)} %get-tuple-element.10), kind=kOutput, calls=%fused_computation.34 | convolution fusion | flops 201621504 | bytes 2623488 | tf_op jit(solution)/shard_map/dot_general | solution.py:601
  179.4 2.7 %fusion.1 = bf16[128,2048]{1,0:T(8,128)(2,1)} fusion(f32[128,2048]{1,0:T(8,128)S(1)} %copy-done.2, f32[128,2048]{1,0:T(8,128)S(1)} %fusion.26, bf16[384,2048]{1,0:T(8,128)(2,1)} %bitcast.14, f32[128]{0:T(128)S(1)} %get-tuple-element.9, s32[128]{0:T(128)S(1)} %get-tuple-element.11, f32[128]{0:T(128)S(1)} %get-tuple-element.8, s32[128]{0:T(128)S(1)} %get-tuple-element.10), kind=kOutput, calls=%fused_computation.3 | convolution fusion | flops 202555392 | bytes 4196352 | tf_op jit(solution)/shard_map/dot_general | solution.py:601
  (14 shorter events, 0.1 us)
Async XLA Ops:
  0.6 162.3 %copy-start = (bf16[512,2048]{1,0:T(8,128)(2,1)S(1)}, bf16[512,2048]{1,0:T(8,128)(2,1)}, u32[]{:S(2)}) copy-start(bf16[512,2048]{1,0:T(8,128)(2,1)} %param.35) | copy-start | bytes 6291460
  0.6 5.7 %copy-start.1 = (bf16[128,2048]{1,0:T(8,128)(2,1)S(1)}, bf16[128,2048]{1,0:T(8,128)(2,1)}, u32[]{:S(2)}) copy-start(bf16[128,2048]{1,0:T(8,128)(2,1)} %param.26) | copy-start | bytes 1572868
  8.9 5.3 %copy-start.5 = (f32[128,2]{0,1:T(2,128)S(1)}, f32[128,2]{0,1:T(2,128)}, u32[]{:S(2)}) copy-start(f32[128,2]{0,1:T(2,128)} %param.29) | copy-start | bytes 3076
  8.9 6.9 %copy-start.3 = (bf16[2,2048,64]{1,2,0:T(8,128)(2,1)S(1)}, bf16[2,2048,64]{1,2,0:T(8,128)(2,1)}, u32[]{:S(2)}) copy-start(bf16[2,2048,64]{1,2,0:T(8,128)(2,1)} %param.32) | copy-start | bytes 1572868
  8.9 135.9 %all-to-all-start = ((bf16[4,96,2048]{2,1,0:T(8,128)(2,1)}), bf16[4,96,2048]{2,1,0:T(8,128)(2,1)}, u32[]{:S(2)}, u32[]{:S(2)}) async-start(bf16[4,96,2048]{2,1,0:T(8,128)(2,1)} %bitcast.34), calls=%async_computation | async-start | bytes 3145728 | tf_op jit(solution)/shard_map/all_to_all | solution.py:570
  152.9 24.5 %all-to-all-start.1 = ((bf16[4,96,2048]{2,1,0:T(8,128)(2,1)}), bf16[4,96,2048]{2,1,0:T(8,128)(2,1)}, u32[]{:S(2)}, u32[]{:S(2)}) async-start(bf16[4,96,2048]{2,1,0:T(8,128)(2,1)} %bitcast.33), calls=%async_computation.1 | async-start | bytes 3145728 | tf_op jit(solution)/shard_map/all_to_all | solution.py:594
  157.3 3.5 %copy-start.4 = (f32[2048]{0:T(1024)S(1)}, f32[2048]{0:T(1024)}, u32[]{:S(2)}) copy-start(f32[2048]{0:T(1024)} %param.27) | copy-start | bytes 24580
  177.4 2.0 %copy-start.2 = (f32[128,2048]{1,0:T(8,128)S(1)}, f32[128,2048]{1,0:T(8,128)}, u32[]{:S(2)}) copy-start(f32[128,2048]{1,0:T(8,128)} %fusion.5) | copy-start | bytes 3145732
